TPU v7x, 512 devices: a whole 4x8x8 slice. The times are simulated.
512 devices in a mesh: sp: 32 (over z, x), dp: 16 (over y, core).
Axes of the slice: x: 4, y: 8, z: 8, core: 2. Of those that a mesh axis runs over, the one named last changes fastest.
Arguments:
- queries: bfloat16 [64, 8, 2048, 128], P('dp', None, 'sp'), may hold values from -6 to 6
- keys: bfloat16 [64, 8, 2048, 128], P('dp', None, 'sp'), may hold values from -6 to 6
- values: bfloat16 [64, 8, 2048, 128], P('dp', None, 'sp'), may hold values from -6 to 6
- input_gate: bfloat16 [64, 8, 2048], P('dp', None, 'sp'), may hold values from -6 to 140
- forget_gate: bfloat16 [64, 8, 2048], P('dp', None, 'sp'), may hold values from 0.5 to 11.5
- start_memory: float32 [64, 8, 128, 128], P('dp', None, 'sp'), may hold values from -6 to 6
- start_norm: float32 [64, 8, 128], P('dp', None, 'sp'), may hold values from -24 to 24
- start_level: float32 [64, 8], P('dp'), may hold values from 2 to 4
- head_gain: float32 [8, 128], replicated, may hold values from 0.1 to 1.9
- out_weight: bfloat16 [1024, 4096], P(None, 'dp'), may hold values from -0.1875 to 0.1875
Outputs:
- mixed: bfloat16 [64, 2048, 4096], P('dp', 'sp')
All inputs are finite; a program needn't handle non-finite values.
Results may differ from a plain program's by a relative error of at most 0.019.
Values may be sent and summed in bfloat16 or wider, within the bound.
A program may use at most 64 MiB of HBM per device.

v0:
```python
import math

import jax
import jax.numpy as jnp
from jax import lax
from jax.sharding import Mesh
from jax.sharding import PartitionSpec as P

BLOCK = 64
SP = ("sp_0", "sp_1")


negative_fill = -1e30


def in_one_piece(arrays, axis, split_dim, concat_dim, along):
    widths = [math.prod(a.shape[along:]) for a in arrays]
    both = jnp.concatenate(
        [a.reshape(*a.shape[:along], w) for a, w in zip(arrays, widths)], axis=along
    )
    result = lax.all_to_all(both, axis, split_axis=split_dim, concat_axis=concat_dim, tiled=True)
    parts = jnp.split(result, [sum(widths[:k]) for k in range(1, len(widths))], axis=along)
    return tuple(
        (b.reshape(*result.shape[:along], *a.shape[along:]) for a, b in zip(arrays, parts))
    )


def in_blocks(x, dim, count):
    dims = x.shape
    parts = x.reshape(*dims[:dim], count, dims[dim] // count, *dims[dim + 1 :])
    return jnp.moveaxis(parts, dim, 0)


def in_order(parts, dim):
    parts = jnp.moveaxis(parts, 0, dim)
    dims = parts.shape
    return parts.reshape(*dims[:dim], dims[dim] * dims[dim + 1], *dims[dim + 2 :])


def exchange_in_order(parts, axes, order):
    dims = [lax.axis_size(a) for a in axes]
    parts = parts.reshape(*dims, *parts.shape[1:])
    for k in order:
        parts = lax.all_to_all(parts, axes[k], split_axis=k, concat_axis=k, tiled=True)
    return parts.reshape(-1, *parts.shape[len(axes) :])


def one_axis_at_a_time(x, axes, order, split_dim, concat_dim):
    parts = in_blocks(x, split_dim, lax.axis_size(axes))
    return in_order(exchange_in_order(parts, axes, order), concat_dim)


def cell_scan(query, key_in, value, input_pre, forget_pre, memory, normal, stabilizer):
    item_count, length, head_width = query.shape
    blocks = length // BLOCK
    factor = head_width ** (-0.5)

    def blocked(tensor):
        return jnp.moveaxis(tensor.reshape((item_count, blocks, BLOCK) + tensor.shape[2:]), 1, 0)

    inputs = (
        blocked(query),
        blocked(key_in),
        blocked(value),
        blocked(input_pre.astype(jnp.float32)),
        blocked(jax.nn.log_sigmoid(forget_pre.astype(jnp.float32))),
    )
    causal = jnp.tril(jnp.ones((BLOCK, BLOCK), dtype=bool))

    def advance(state, block_data):
        memory, normal, stabilizer = state
        query_block, key_block, value_block, gate_in, gate_keep = block_data
        scaled = query_block.astype(jnp.float32) * factor
        cumulative = jnp.cumsum(gate_keep, axis=-1)
        logits = jnp.where(
            causal,
            cumulative[:, :, None] - cumulative[:, None, :] + gate_in[:, None, :],
            negative_fill,
        )
        carried = cumulative + stabilizer[:, None]
        running_max = jnp.maximum(carried, jnp.max(logits, axis=-1))
        raw = (
            jnp.einsum("ptd,psd->pts", query_block, key_block, preferred_element_type=jnp.float32)
            * factor
        )
        scores = raw * jnp.exp(logits - running_max[..., None])
        rounded = scores.astype(jnp.bfloat16)
        carry_weight = jnp.exp(carried - running_max)
        numerator = jnp.einsum(
            "pts,pse->pte", rounded, value_block, preferred_element_type=jnp.float32
        ) + carry_weight[..., None] * jnp.einsum("ptd,pde->pte", scaled, memory)
        denominator = jnp.sum(scores, axis=-1) + carry_weight * jnp.einsum(
            "ptd,pd->pt", scaled, normal
        )
        output = numerator / jnp.maximum(jnp.abs(denominator), 1.0)[..., None]
        block_total = cumulative[:, -1]
        weights_log = block_total[:, None] - cumulative + gate_in
        stabilizer_new = jnp.maximum(block_total + stabilizer, jnp.max(weights_log, axis=-1))
        weights = jnp.exp(weights_log - stabilizer_new[:, None])
        shrink = jnp.exp(block_total + stabilizer - stabilizer_new)
        weighted = key_block.astype(jnp.float32) * weights[..., None]
        packed = weighted.astype(jnp.bfloat16)
        memory_new = shrink[:, None, None] * memory + jnp.einsum(
            "psd,pse->pde", packed, value_block, preferred_element_type=jnp.float32
        )
        normal_new = shrink[:, None] * normal + jnp.sum(weighted, axis=1)
        return ((memory_new, normal_new, stabilizer_new), output)

    start = (memory.astype(jnp.float32), normal.astype(jnp.float32), stabilizer)
    _, outputs = lax.scan(advance, start, inputs)
    return jnp.moveaxis(outputs, 0, 1).reshape(item_count, length, head_width).astype(jnp.bfloat16)


def normalize(hidden, gain):
    entries = hidden.astype(jnp.float32)
    return (entries * gain[:, None, :]).astype(jnp.bfloat16)


def on_device(
    queries,
    keys,
    values,
    input_gate,
    forget_gate,
    start_memory,
    start_norm,
    start_level,
    head_gain,
    out_weight,
):
    local_seqs, heads, tokens_here, head_width = queries.shape
    count = local_seqs * heads
    group_size = lax.axis_size(SP)
    owned_items = count // group_size

    def to_items(tensor):
        return tensor.reshape((count,) + tensor.shape[2:])

    received = (
        lax.all_to_all(to_items(queries), SP, split_axis=0, concat_axis=1, tiled=True),
        lax.all_to_all(to_items(keys), SP, split_axis=0, concat_axis=1, tiled=True),
        lax.all_to_all(to_items(values), SP, split_axis=0, concat_axis=1, tiled=True),
        lax.all_to_all(to_items(input_gate), SP, split_axis=0, concat_axis=1, tiled=True),
        lax.all_to_all(to_items(forget_gate), SP, split_axis=0, concat_axis=1, tiled=True),
    )
    memory, normal = tuple(
        (
            part.astype(jnp.float32)
            for part in in_one_piece(
                (
                    to_items(start_memory).astype(jnp.bfloat16),
                    to_items(start_norm).astype(jnp.bfloat16),
                ),
                SP,
                0,
                1,
                2,
            )
        )
    )
    stabilizer = lax.dynamic_slice_in_dim(
        start_level.reshape(count), lax.axis_index(SP) * owned_items, owned_items
    )
    hidden = cell_scan(
        received[0], received[1], received[2], received[3], received[4], memory, normal, stabilizer
    )
    returned = one_axis_at_a_time(hidden, SP, (0, 1), 1, 0).reshape(
        local_seqs, heads, tokens_here, head_width
    )
    normed = normalize(returned, head_gain)
    block_data = lax.all_gather(out_weight, "dp", axis=1, tiled=True)
    shaped = block_data.reshape(heads, head_width, block_data.shape[1])
    return jnp.einsum("shtd,hdc->stc", normed, shaped, preferred_element_type=jnp.float32).astype(
        jnp.bfloat16
    )


def solution(mesh):
    split = Mesh(mesh.devices.reshape(8, 4, mesh.shape["dp"]), ("sp_0", "sp_1", "dp"))
    return jax.shard_map(
        on_device,
        mesh=split,
        in_specs=(
            P("dp", None, SP, None),
            P("dp", None, SP, None),
            P("dp", None, SP, None),
            P("dp", None, SP),
            P("dp", None, SP),
            P("dp", None, SP, None),
            P("dp", None, SP),
            P("dp", None),
            P(),
            P(None, "dp"),
        ),
        out_specs=P("dp", SP, None),
        check_vma=False,
    )
```

profile of v0, /device:TPU:56, one launch (start us, length us, event | category | flops | bytes accessed | tf_op | source)
XLA Modules:
  0.0 346.6 jit_solution(8085328857293592038)
XLA Ops:
  6.5 1.3 copy.30
  7.9 13.2 %all-to-all-start.1 = ((bf16[32,1,64]{2,1,0:T(2,128)(2,1)}), bf16[32,1,64]{2,1,0:T(2,128)(2,1)S(1)}, u32[]{:S(2)}, u32[]{:S(2)}) async-start(bf16[32,1,64]{2,1,0:T(2,128)(2,1)} %copy.30), calls=%async_computation.1 | async-start | bytes 32768 | tf_op jit(solution)/shard_map/all_to_all | solution.py:144
  22.8 1.3 copy.32
  24.1 6.6 %all-to-all-done.1 = bf16[32,1,64]{2,1,0:T(2,128)(2,1)S(1)} async-done(((bf16[32,1,64]{2,1,0:T(2,128)(2,1)}), bf16[32,1,64]{2,1,0:T(2,128)(2,1)S(1)}, u32[]{:S(2)}, u32[]{:S(2)}) %all-to-all-start.1) | async-done | bytes 4128 | tf_op jit(solution)/shard_map/all_to_all | solution.py:144
  30.7 3.9 %all-to-all-start.2 = ((bf16[32,1,64]{2,1,0:T(2,128)(2,1)}), bf16[32,1,64]{2,1,0:T(2,128)(2,1)S(1)}, u32[]{:S(2)}, u32[]{:S(2)}) async-start(bf16[32,1,64]{2,1,0:T(2,128)(2,1)} %copy.32), calls=%async_computation.2 | async-start | bytes 32768 | tf_op jit(solution)/shard_map/all_to_all | solution.py:143
  34.6 9.6 %all-to-all-done.2 = bf16[32,1,64]{2,1,0:T(2,128)(2,1)S(1)} async-done(((bf16[32,1,64]{2,1,0:T(2,128)(2,1)}), bf16[32,1,64]{2,1,0:T(2,128)(2,1)S(1)}, u32[]{:S(2)}, u32[]{:S(2)}) %all-to-all-start.2) | async-done | bytes 4128 | tf_op jit(solution)/shard_map/all_to_all | solution.py:143
  44.2 12.9 %all_to_all.84 = bf16[32,4,129]{2,1,0:T(4,128)(2,1)S(1)} all-to-all(bf16[32,4,129]{2,1,0:T(4,128)(2,1)S(1)} %pad_maximum_fusion), channel_id=1, replica_groups=mesh['sp_0'=8,'sp_1'=4,'dp'=16] {'sp_0','sp_1'}, dimensions={0} | all-to-all | bytes 66048 | tf_op jit(solution)/shard_map/all_to_all | solution.py:21
  57.1 18.9 %all_to_all.85 = bf16[32,64,128]{2,1,0:T(8,128)(2,1)S(1)} all-to-all(bf16[32,64,128]{2,1,0:T(8,128)(2,1)} %bitcast.188), channel_id=1, replica_groups=mesh['sp_0'=8,'sp_1'=4,'dp'=16] {'sp_0','sp_1'}, dimensions={0} | all-to-all | bytes 1048576 | tf_op jit(solution)/shard_map/all_to_all | solution.py:141
  76.0 18.5 %all_to_all.86 = bf16[32,64,128]{2,1,0:T(8,128)(2,1)S(1)} all-to-all(bf16[32,64,128]{2,1,0:T(8,128)(2,1)} %bitcast.189), channel_id=1, replica_groups=mesh['sp_0'=8,'sp_1'=4,'dp'=16] {'sp_0','sp_1'}, dimensions={0} | all-to-all | bytes 1048576 | tf_op jit(solution)/shard_map/all_to_all | solution.py:142
  94.5 4.2 %all-to-all-start.5 = ((bf16[32,64,128]{2,1,0:T(8,128)(2,1)}), bf16[32,64,128]{2,1,0:T(8,128)(2,1)S(1)}, u32[]{:S(2)}, u32[]{:S(2)}) async-start(bf16[32,64,128]{2,1,0:T(8,128)(2,1)} %bitcast.190), calls=%async_computation.5 | async-start | bytes 1048576 | tf_op jit(solution)/shard_map/all_to_all | solution.py:140
  101.0 11.5 %all-to-all-done.5 = bf16[32,64,128]{2,1,0:T(8,128)(2,1)S(1)} async-done(((bf16[32,64,128]{2,1,0:T(8,128)(2,1)}), bf16[32,64,128]{2,1,0:T(8,128)(2,1)S(1)}, u32[]{:S(2)}, u32[]{:S(2)}) %all-to-all-start.5) | async-done | bytes 524320 | tf_op jit(solution)/shard_map/all_to_all | solution.py:140
  112.5 193.3 %while.17 = (s32[]{:T(128)}, f32[1,128,128]{2,1,0:T(8,128)S(1)}, f32[1,128]{1,0:T(1,128)S(1)}, f32[1]{0:T(128)}, bf16[32,1,64,128]{3,2,1,0:T(8,128)(2,1)S(1)}, /...) while((s32[]{:T(128)}, f32[1,128,128]{2,1,0:T(8,128)S(1)}, ...), condition=%wide.region_6.7_spmd.clone, body=%wide.region_0.6_spmd.clone.sunk | while | flops 6509316 | bytes 466661 | solution.py:110
  113.3 1.2 fusion.94
  119.3 1.2 fusion.94
  125.4 1.2 fusion.94
  131.4 1.2 fusion.94
  137.5 1.2 fusion.94
  155.6 1.2 fusion.94
  161.6 1.2 fusion.94
  167.7 1.2 fusion.94
  173.7 1.2 fusion.94
  305.8 16.2 %all_to_all.87 = bf16[8,4,1,64,128]{4,3,1,2,0:T(8,128)(2,1)S(1)} all-to-all(bf16[8,4,1,64,128]{4,3,1,2,0:T(8,128)(2,1)S(1)} %bitcast.192), channel_id=1, replica_groups=mesh['sp_0'=8,'sp_1'=4,'dp'=16] {'sp_0'}, dimensions={0} | all-to-all | bytes 1048576 | tf_op jit(solution)/shard_map/all_to_all | solution.py:44
  322.0 10.8 %all_to_all.88 = bf16[8,4,1,64,128]{4,3,0,2,1:T(8,128)(2,1)S(1)} all-to-all(bf16[8,4,1,64,128]{4,3,0,2,1:T(8,128)(2,1)S(1)} %copy.34), channel_id=1, replica_groups=mesh['sp_0'=8,'sp_1'=4,'dp'=16] {'sp_1'}, dimensions={1} | all-to-all | bytes 1048576 | tf_op jit(solution)/shard_map/all_to_all | solution.py:44
  332.9 6.9 %fusion.49 = bf16[4,64,4096]{2,1,0:T(8,128)(2,1)} fusion(bf16[8,128,4096,1]{2,1,0,3:T(8,128)(2,1)} %bitcast.201, bf16[4,8,64,128]{3,2,1,0:T(8,128)(2,1)S(1)} %bitcast.193, f32[8,128]{1,0:T(8,128)S(1)} %copy-done), kind=kOutput, calls=%fused_computation.64 | convolution fusion | flops 2149318656 | bytes 11014144 | tf_op jit(solution)/shard_map/shtd,hdc->stc/dot_general | solution.py:173
  (459 shorter events, 111.1 us)
Async XLA Ops:
  6.5 326.3 %copy-start = (f32[8,128]{1,0:T(8,128)S(1)}, f32[8,128]{1,0:T(8,128)}, u32[]{:S(2)}) copy-start(f32[8,128]{1,0:T(8,128)} %param.20) | copy-start | bytes 12292
  7.9 22.9 %all-to-all-start.1 = ((bf16[32,1,64]{2,1,0:T(2,128)(2,1)}), bf16[32,1,64]{2,1,0:T(2,128)(2,1)S(1)}, u32[]{:S(2)}, u32[]{:S(2)}) async-start(bf16[32,1,64]{2,1,0:T(2,128)(2,1)} %copy.30), calls=%async_computation.1 | async-start | bytes 32768 | tf_op jit(solution)/shard_map/all_to_all | solution.py:144
  30.7 13.5 %all-to-all-start.2 = ((bf16[32,1,64]{2,1,0:T(2,128)(2,1)}), bf16[32,1,64]{2,1,0:T(2,128)(2,1)S(1)}, u32[]{:S(2)}, u32[]{:S(2)}) async-start(bf16[32,1,64]{2,1,0:T(2,128)(2,1)} %copy.32), calls=%async_computation.2 | async-start | bytes 32768 | tf_op jit(solution)/shard_map/all_to_all | solution.py:143
  94.5 18.0 %all-to-all-start.5 = ((bf16[32,64,128]{2,1,0:T(8,128)(2,1)}), bf16[32,64,128]{2,1,0:T(8,128)(2,1)S(1)}, u32[]{:S(2)}, u32[]{:S(2)}) async-start(bf16[32,64,128]{2,1,0:T(8,128)(2,1)} %bitcast.190), calls=%async_computation.5 | async-start | bytes 1048576 | tf_op jit(solution)/shard_map/all_to_all | solution.py:140
  98.7 234.2 %all-gather.2.cloned.1.call-start = ((), (), s32[]{:S(2)}) async-start(), calls=%async_computation.8 | async-start | bytes 8912896 | tf_op jit(solution)/shard_map/all_gather | solution.py:171
Sparse Core Ops, SparseCore 0:
  101.5 66.6 all-gather.1
where the time goes:
time: 349 us; the launch traced here: 347 us
  blocking collectives  77.2 us (22%)
  loops' own time  75.8 us (22%)
  other arithmetic  72.7 us (21%)
  matrix products  35.6 us (10%)
  waiting for transfers between devices  28.4 us (8%)
  local copies, waits for them, and re-layouts  22.2 us (6%)
  starting transfers between devices  21.2 us (6%)
  between operations  13.5 us (4%)
    another operation x1, loops' own time, cell_scan(): _, outputs = lax.scan(advance, start, inputs)  75.8 us
    reduce_max x32, other arithmetic, advance(): jnp.max(weights_log, axis=-1)  37.6 us
    all_to_all x2, blocking collectives, exchange_in_order(): lax.all_to_all(parts, axes[k], split_axis=k, concat_axis=k, tiled=True)  26.9 us
    all_to_all x1, blocking collectives, on_device(): lax.all_to_all(to_items(keys), SP, split_axis=0, concat_axis=1, tiled=True)  18.9 us
    all_to_all x1, blocking collectives, on_device(): lax.all_to_all(to_items(values), SP, split_axis=0, concat_axis=1, tiled=T...  18.5 us
    exp x32, other arithmetic, advance(): weights = jnp.exp(weights_log - stabilizer_new[:, None])  18.5 us
    slice x32, local copies, waits for them, and re-layouts, advance(): block_total = cumulative[:, -1]  17.8 us
    all_to_all x1, starting transfers between devices, on_device(): lax.all_to_all(to_items(forget_gate), SP, split_axis=0, concat_axis=1, ti...  13.2 us
  transfers between devices with their start and end apart: 4, of which 3 were waited for; matrix products, arithmetic and copies ran while one was open for 35% of the time, Pallas kernels for 0%

commit v1 on v0

v1 whole, which is shorter than its diff:
```python
import jax
import jax.numpy as jnp
from jax import lax
from jax.experimental import pallas as pl
from jax.experimental.pallas import tpu as pltpu
from jax.sharding import PartitionSpec as P

MESH = pl.DeviceIdType.MESH
F32 = jnp.float32
BF16 = jnp.bfloat16
S, H, T, D = 4, 8, 64, 128
NX, NZ, NY = 4, 8, 8
FACTOR = D**-0.5
NEG = -1e30
CH = 4
CROWS = 1024 // CH
LAST = 3 * CH + CH // 2


def nt(a, b):
    return lax.dot_general(a, b, (((1,), (1,)), ((), ())), preferred_element_type=F32)


def kernel(
    g_hbm, q_hbm, k_hbm, v_hbm, c_hbm, w_hbm, level, gain, out_hbm,
    qv, kv, vv, gv, cv, kx, vx, gx, cx, wall, a_loc, num_s, den_s, amx_s,
    wrow, esum, amax, kvs, nkv, cz_send, cz_recv, t_send, t_recv, tm_send, tm_recv,
    p_send, p_recv, pm_send, pm_recv, b_send, b_recv, bm_send, bm_recv, hid, ob,
    lsem, xin_s, xin_r, cz_s, cz_r, tz_s, tz_r, pz_s, pz_r, xo_s, xo_r,
    wy_s, wy_r, wd_s, wd_r, wo_s, wo_r, osem,
):
    sp = lax.axis_index("sp")
    dp = lax.axis_index("dp")
    x, z = lax.rem(sp, NX), lax.div(sp, NX)
    y, c = lax.div(dp, 2), lax.rem(dp, 2)

    def xdev(d):
        return {"sp": z * NX + lax.rem(x + d, NX), "dp": dp}

    def zdev(d):
        return {"sp": lax.rem(z + d, NZ) * NX + x, "dp": dp}

    def ydev(d):
        return {"sp": sp, "dp": lax.rem(y + d + NY, NY) * 2 + c}

    mate = {"sp": sp, "dp": y * 2 + (1 - c)}

    def remote(src, dst, ssem, rsem, dev):
        return pltpu.make_async_remote_copy(
            src_ref=src, dst_ref=dst, send_sem=ssem, recv_sem=rsem,
            device_id=dev, device_id_type=MESH,
        )

    loads = [
        pltpu.make_async_copy(g_hbm, gv, lsem.at[0]),
        pltpu.make_async_copy(k_hbm, kv, lsem.at[1]),
        pltpu.make_async_copy(v_hbm, vv, lsem.at[2]),
        pltpu.make_async_copy(w_hbm, wall.at[dp], lsem.at[3]),
        pltpu.make_async_copy(c_hbm, cv, lsem.at[4]),
        pltpu.make_async_copy(q_hbm, qv, lsem.at[5]),
        pltpu.make_async_copy(k_hbm.at[x], kx.at[x], lsem.at[6]),
        pltpu.make_async_copy(v_hbm.at[x], vx.at[x], lsem.at[7]),
        pltpu.make_async_copy(g_hbm.at[x], gx.at[x], lsem.at[8]),
        pltpu.make_async_copy(c_hbm.at[x], cx.at[x], lsem.at[9]),
    ]
    for load in loads:
        load.start()

    barrier = pltpu.get_barrier_semaphore()
    peers = [xdev(d) for d in range(1, NX)] + [zdev(d) for d in range(1, NZ)]
    peers += [ydev(1), ydev(-1), mate]
    for dev in peers:
        pl.semaphore_signal(barrier, inc=1, device_id=dev, device_id_type=MESH)

    rows64 = lax.broadcasted_iota(jnp.int32, (T, T), 0)
    cols64 = lax.broadcasted_iota(jnp.int32, (T, T), 1)
    upper = jnp.where(rows64 <= cols64, 1.0, 0.0).astype(F32)
    causal = rows64 >= cols64

    def gates(g):
        li = g[0:8, 0:T]
        f = g[8:16, 0:T]
        lf = jnp.minimum(f, 0.0) - jnp.log1p(jnp.exp(-jnp.abs(f)))
        b = jnp.dot(lf, upper, precision=lax.Precision.HIGHEST, preferred_element_type=F32)
        return li - b, b[:, T - 1 : T]

    for load in loads:
        load.wait()
    for j in range(S):
        a, _ = gates(gv[j])
        a_loc[8 * j : 8 * j + 8, :] = a

    pl.semaphore_wait(barrier, len(peers))

    def wpart(by, bc, part):
        return wall.at[by * 2 + bc, pl.ds(part * CROWS, CROWS), :]

    def part_of(side, n):
        return (n + side * CH // 2) % CH

    def wchunk(side, n):
        by = lax.rem(y - 1 - n // CH + 2 * NY, NY) if side == 0 else lax.rem(y + 1 + n // CH, NY)
        return wpart(by, c, part_of(side, n))

    def wsend(side, n):
        if n < CH:
            ref = wpart(y, c, part_of(side, n))
        else:
            ref = wchunk(side, n - CH)
        return remote(ref, ref, wy_s.at[side, n], wy_r.at[side, n], ydev(1 if side == 0 else -1))

    def xin(d):
        p = lax.rem(x + d, NX)
        dev = xdev(d)
        i = d - 1
        return [
            remote(gv.at[p], gx.at[x], xin_s.at[0, i], xin_r.at[0, i], dev),
            remote(kv.at[p], kx.at[x], xin_s.at[1, i], xin_r.at[1, i], dev),
            remote(vv.at[p], vx.at[x], xin_s.at[2, i], xin_r.at[2, i], dev),
            remote(cv.at[p], cx.at[x], xin_s.at[3, i], xin_r.at[3, i], dev),
        ]

    def xin_recv(d):
        p = lax.rem(x - d + NX, NX)
        dev = xdev(d)
        i = d - 1
        return [
            remote(gv.at[0], gx.at[p], xin_s.at[0, i], xin_r.at[0, i], dev),
            remote(kv.at[0], kx.at[p], xin_s.at[1, i], xin_r.at[1, i], dev),
            remote(vv.at[0], vx.at[p], xin_s.at[2, i], xin_r.at[2, i], dev),
            remote(cv.at[0], cx.at[p], xin_s.at[3, i], xin_r.at[3, i], dev),
        ]

    for d in (2, 1, 3):
        for copy in xin(d):
            copy.start()
    for n in range(CH):
        wsend(0, n).start()
        wsend(1, n).start()
    w_own = remote(wall.at[dp], wall.at[dp], wo_s.at[0], wo_r.at[0], mate)
    w_own.start()

    def serve(n):
        for side in (0, 1):
            ref = wchunk(side, n)
            remote(ref, ref, wy_s.at[side, n], wy_r.at[side, n], ydev(1)).wait_recv()
            if n + CH < LAST:
                wsend(side, n + CH).start()
            remote(ref, ref, wd_s.at[side, n], wd_r.at[side, n], mate).start()

    def intra(i, _):
        j, h = lax.div(i, H), lax.rem(i, H)
        arow = a_loc[pl.ds(i, 1), :]
        masked = jnp.where(causal, jnp.broadcast_to(arow, (T, T)), NEG)
        top = jnp.max(masked, axis=1, keepdims=True)
        weight = jnp.exp(masked - top)
        scores = nt(qv[j, h], kv[j, h]) * FACTOR * weight
        den_s[i] = jnp.broadcast_to(jnp.sum(scores, axis=1, keepdims=True), (T, D))
        amx_s[i] = jnp.broadcast_to(top, (T, D))
        num_s[i] = jnp.dot(scores.astype(BF16), vv[j, h], preferred_element_type=F32)
        return 0

    def pairs(fn, count):
        def body(i, _):
            for u in range(4):
                fn(i * 4 + u, 0)
            return 0

        lax.fori_loop(0, count // 4, body, 0)

    pairs(intra, S * H)

    def block_states(p):
        a, e = gates(gx[p])
        am = jnp.max(a, axis=1, keepdims=True)
        esum[p] = jnp.broadcast_to(e, (H, D))
        amax[p] = jnp.broadcast_to(am, (H, D))
        wrow[...] = jnp.exp(a - am)

        def one(h, _):
            w = wrow[pl.ds(h, 1), :]
            vt = vx[p, h].astype(F32).T
            hi = w.astype(BF16)
            lo = (w - hi.astype(F32)).astype(BF16)
            rid = lax.broadcasted_iota(jnp.int32, (16, T), 0)
            extra = jnp.where(
                rid == 0,
                jnp.broadcast_to(hi.astype(F32), (16, T)),
                jnp.where(rid == 1, jnp.broadcast_to(lo.astype(F32), (16, T)), 0.0),
            )
            lhs = jnp.concatenate([(vt * w).astype(BF16), extra.astype(BF16)], axis=0)
            st = jnp.dot(lhs, kx[p, h], preferred_element_type=F32)
            kvs[p, h] = st[0:D]
            nkv[p, pl.ds(h, 1), :] = st[D : D + 1] + st[D + 1 : D + 2]
            return 0

        pairs(one, H)

    block_states(x)
    serve(0)
    for count, d in enumerate((1, 3, 2)):
        for copy in xin_recv(d):
            copy.wait_recv()
        block_states(lax.rem(x - d + NX, NX))
        serve(1 + count)

    for i in range(NX):
        for h in range(H):
            cz_send[h, 4 * i : 4 * i + 4, :] = cx[i, 4 * h : 4 * h + 4, :]

    shift = []
    before = jnp.zeros((H, D), F32)
    top = None
    for i in range(NX):
        a = amax[i] - before
        shift.append(a)
        top = a if top is None else jnp.maximum(top, a)
        before = before + esum[i]
    scale = [jnp.exp(a - top) for a in shift]
    ntot = sum(scale[i] * nkv[i] for i in range(NX))
    n0 = sum(gx[i, 16:24, :] for i in range(NX))
    for h in range(H):
        tm_send[h, 0:1, :] = ntot[h : h + 1]
        tm_send[h, 1:2, :] = before[h : h + 1]
        tm_send[h, 2:3, :] = top[h : h + 1]
        tm_send[h, 3:4, :] = n0[h : h + 1]
        t_send[h] = sum(scale[i][h : h + 1] * kvs[i, h] for i in range(NX)).astype(BF16)

    def tz(d):
        p = lax.rem(z + d, NZ)
        dev = zdev(d)
        i = d - 1
        return [
            remote(cz_send.at[p], cz_recv.at[z], tz_s.at[2, i], tz_r.at[2, i], dev),
            remote(tm_send.at[p], tm_recv.at[z], tz_s.at[0, i], tz_r.at[0, i], dev),
            remote(t_send.at[p], t_recv.at[z], tz_s.at[1, i], tz_r.at[1, i], dev),
        ]

    def tz_recv(d):
        p = lax.rem(z - d + NZ, NZ)
        dev = zdev(d)
        i = d - 1
        return [
            remote(cz_send.at[0], cz_recv.at[p], tz_s.at[2, i], tz_r.at[2, i], dev),
            remote(tm_send.at[0], tm_recv.at[p], tz_s.at[0, i], tz_r.at[0, i], dev),
            remote(t_send.at[0], t_recv.at[p], tz_s.at[1, i], tz_r.at[1, i], dev),
        ]

    for d in (4, 3, 5, 2, 6, 1, 7):
        for copy in tz(d):
            copy.start()
    t_recv[z] = t_send[z]
    tm_recv[z] = tm_send[z]
    cz_recv[z] = cz_send[z]
    serve(4)
    for d in (1, 7, 2, 6, 3, 5, 4):
        for copy in tz_recv(d):
            copy.wait_recv()

    m = jnp.full((1, D), level[x, z], F32)
    nrow = sum(tm_recv[i, 3:4, :] for i in range(NZ))
    state = jnp.concatenate([cz_recv[i] for i in range(NZ)], axis=0).T
    for i in range(NZ):
        p_send[i] = state.astype(BF16)
        pm_send[i, 0:1, :] = nrow
        pm_send[i, 1:2, :] = m
        am = tm_recv[i, 2:3, :]
        hi = jnp.maximum(m, am)
        keep, add = jnp.exp(m - hi), jnp.exp(am - hi)
        state = keep * state + add * t_recv[i].astype(F32)
        nrow = keep * nrow + add * tm_recv[i, 0:1, :]
        m = tm_recv[i, 1:2, :] + hi

    def pz(d):
        p = lax.rem(z + d, NZ)
        dev = zdev(d)
        i = d - 1
        return [
            remote(pm_send.at[p], pm_recv.at[z], pz_s.at[0, i], pz_r.at[0, i], dev),
            remote(p_send.at[p], p_recv.at[z], pz_s.at[1, i], pz_r.at[1, i], dev),
        ]

    def pz_recv(d):
        p = lax.rem(z - d + NZ, NZ)
        dev = zdev(d)
        i = d - 1
        return [
            remote(pm_send.at[0], pm_recv.at[p], pz_s.at[0, i], pz_r.at[0, i], dev),
            remote(p_send.at[0], p_recv.at[p], pz_s.at[1, i], pz_r.at[1, i], dev),
        ]

    for d in (4, 3, 5, 2, 6, 1, 7):
        for copy in pz(d):
            copy.start()
    p_recv[z] = p_send[z]
    pm_recv[z] = pm_send[z]
    serve(5)
    serve(6)
    for d in (1, 7, 2, 6, 3, 5, 4):
        for copy in pz_recv(d):
            copy.wait_recv()
    serve(7)

    for h in range(H):
        state = p_recv[h].astype(F32)
        nrow = pm_recv[h, 0:1, :]
        m = pm_recv[h, 1:2, :]
        for i in range(NX):
            b_send[i, h] = state.astype(BF16)
            bm_send[i, h : h + 1, :] = nrow
            bm_send[i, H + h : H + h + 1, :] = m
            if i < NX - 1:
                am = amax[i, h : h + 1, :]
                hi = jnp.maximum(m, am)
                keep, add = jnp.exp(m - hi), jnp.exp(am - hi)
                state = keep * state + add * kvs[i, h]
                nrow = keep * nrow + add * nkv[i, h : h + 1, :]
                m = esum[i, h : h + 1, :] + hi

    def xo(d):
        p = lax.rem(x + d, NX)
        dev = xdev(d)
        i = d - 1
        return [
            remote(bm_send.at[p], bm_recv.at[x], xo_s.at[0, i], xo_r.at[0, i], dev),
            remote(b_send.at[p], b_recv.at[x], xo_s.at[1, i], xo_r.at[1, i], dev),
        ]

    def xo_recv(d):
        p = lax.rem(x - d + NX, NX)
        dev = xdev(d)
        i = d - 1
        return [
            remote(bm_send.at[0], bm_recv.at[p], xo_s.at[0, i], xo_r.at[0, i], dev),
            remote(b_send.at[0], b_recv.at[p], xo_s.at[1, i], xo_r.at[1, i], dev),
        ]

    for d in (2, 1, 3):
        for copy in xo(d):
            copy.start()
    b_recv[x] = b_send[x]
    bm_recv[x] = bm_send[x]

    def finish(j):
        def one(h, _):
            i = j * H + h
            q = qv[j, h]
            nrow = bm_recv[j, pl.ds(h, 1), :]
            m = bm_recv[j, pl.ds(H + h, 1), :]
            qc = nt(q, b_recv[j, h])
            qn = jnp.sum(q.astype(F32) * nrow, axis=1, keepdims=True)
            a = amx_s[i]
            hi = jnp.maximum(a, m)
            keep, add = jnp.exp(m - hi) * FACTOR, jnp.exp(a - hi)
            den = add * den_s[i] + keep * qn
            num = add * num_s[i] + keep * qc
            o = (num / jnp.maximum(jnp.abs(den), 1.0)).astype(BF16)
            normed = (o.astype(F32) * gain[pl.ds(h, 1), :]).astype(BF16)
            hid[pl.ds(pl.multiple_of(j * T, T), T), pl.ds(pl.multiple_of(h * D, D), D)] = normed
            return 0

        pairs(one, H)

    finish(x)
    serve(8)
    for count, d in enumerate((1, 3, 2)):
        for copy in xo_recv(d):
            copy.wait_recv()
        finish(lax.rem(x - d + NX, NX))
        serve(9 + count)
    serve(12)
    serve(13)

    remote(wall.at[dp], wall.at[y * 2 + 1 - c], wo_s.at[0], wo_r.at[0], mate).wait_recv()
    for n in range(LAST):
        for side in (0, 1):
            ref = wchunk(side, n)
            remote(ref, ref, wd_s.at[side, n], wd_r.at[side, n], mate).wait_recv()

    def project(i, _):
        cols = pl.ds(pl.multiple_of(i * 256, 256), 256)
        ob[i] = jnp.dot(hid[...], wall[i], preferred_element_type=F32).astype(BF16)
        pltpu.make_async_copy(ob.at[i], out_hbm.at[:, cols], osem.at[i]).start()
        return 0

    lax.fori_loop(0, 2 * NY, project, 0)

    for i in range(2 * NY):
        pltpu.make_async_copy(ob.at[i], out_hbm.at[:, 256 * i : 256 * i + 256], osem.at[i]).wait()
    for d in range(1, NX):
        for copy in xin(d) + xo(d):
            copy.wait_send()
    for d in range(1, NZ):
        for copy in tz(d) + pz(d):
            copy.wait_send()
    w_own.wait_send()
    for n in range(LAST):
        for side in (0, 1):
            wsend(side, n).wait_send()
            ref = wchunk(side, n)
            remote(ref, ref, wd_s.at[side, n], wd_r.at[side, n], mate).wait_send()


def on_device(queries, keys, values, input_gate, forget_gate, start_memory, start_norm, start_level, head_gain, out_weight):
    sp = lax.axis_index("sp")
    lane = lax.broadcasted_iota(jnp.int32, (S, H, D), 2)
    spread = jnp.where(lane // 4 == sp, jnp.tile(start_norm, (1, 1, D // 4)), 0.0)
    pad = ((0, 0), (0, 0), (0, D - T))
    g = jnp.concatenate(
        [jnp.pad(input_gate.astype(F32), pad), jnp.pad(forget_gate.astype(F32), pad), spread], axis=1
    )
    dma, vmem = pltpu.SemaphoreType.DMA, pltpu.VMEM
    anyspec = pl.BlockSpec(memory_space=pl.ANY)
    out = pl.pallas_call(
        kernel,
        out_shape=jax.ShapeDtypeStruct((S * T, 4096), BF16),
        in_specs=[anyspec] * 6
        + [pl.BlockSpec(memory_space=pltpu.SMEM), pl.BlockSpec(memory_space=pltpu.VMEM)],
        out_specs=anyspec,
        scratch_shapes=[
            vmem((S, H, T, D), BF16), vmem((S, H, T, D), BF16), vmem((S, H, T, D), BF16),
            vmem((S, 24, D), F32), vmem((S, 32, D), F32),
            vmem((NX, H, T, D), BF16), vmem((NX, H, T, D), BF16),
            vmem((NX, 24, D), F32), vmem((NX, 32, D), F32),
            vmem((2 * NY, 1024, 256), BF16),
            vmem((S * H, T), F32),
            vmem((S * H, T, D), F32), vmem((S * H, T, D), F32), vmem((S * H, T, D), F32),
            vmem((H, T), F32), vmem((NX, H, D), F32), vmem((NX, H, D), F32),
            vmem((NX, H, D, D), F32), vmem((NX, H, D), F32),
            vmem((H, 16, D), F32), vmem((NZ, 16, D), F32),
            vmem((H, D, D), BF16), vmem((NZ, D, D), BF16),
            vmem((H, 8, D), F32), vmem((NZ, 8, D), F32),
            vmem((NZ, D, D), BF16), vmem((H, D, D), BF16),
            vmem((NZ, 8, D), F32), vmem((H, 8, D), F32),
            vmem((NX, H, D, D), BF16), vmem((S, H, D, D), BF16),
            vmem((NX, 16, D), F32), vmem((S, 16, D), F32),
            vmem((S * T, H * D), BF16),
            vmem((2 * NY, S * T, 256), BF16),
            dma((10,)),
            dma((4, 3)), dma((4, 3)),
            dma((1,)), dma((1,)),
            dma((3, 7)), dma((3, 7)),
            dma((2, 7)), dma((2, 7)),
            dma((2, 3)), dma((2, 3)),
            dma((2, LAST)), dma((2, LAST)), dma((2, LAST)), dma((2, LAST)),
            dma((1,)), dma((1,)), dma((2 * NY,)),
        ],
        compiler_params=pltpu.CompilerParams(
            collective_id=0, has_side_effects=True, vmem_limit_bytes=48 * 1024 * 1024
        ),
        name="cell_layer",
    )(
        g, queries, keys, values, start_memory.reshape(S, 32, D), out_weight, start_level, head_gain
    )
    return out.reshape(S, T, 4096)


def solution(mesh):
    return jax.shard_map(
        on_device,
        mesh=mesh,
        in_specs=(
            P("dp", None, "sp", None),
            P("dp", None, "sp", None),
            P("dp", None, "sp", None),
            P("dp", None, "sp"),
            P("dp", None, "sp"),
            P("dp", None, "sp", None),
            P("dp", None, "sp"),
            P("dp", None),
            P(),
            P(None, "dp"),
        ),
        out_specs=P("dp", "sp", None),
        check_vma=False,
    )
```

time: 349 us -> 87.7 us (0.25)
  the two profiles are of different devices: /device:TPU:56 before, /device:TPU:1 now
where the time goes in v1:
time: 87.7 us; the launch traced here: 87.3 us
  Pallas kernels  77.9 us (89%)
  local copies, waits for them, and re-layouts  8.51 us (10%)
    pallas_call x1, Pallas kernels, on_device(): pl.pallas_call(kernel, out_shape=jax.ShapeDtypeStruct((S * T, 4096), BF16...  77.9 us
    unnamed x15, local copies, waits for them, and re-layouts  7.69 us

profile of v1, /device:TPU:1, one launch (start us, length us, event | category | flops | bytes accessed | tf_op | source)
XLA Modules:
  0.0 87.3 jit_solution(831862615074378125)
XLA Ops:
  0.0 0.7 pad_convert_fusion
  0.7 0.7 tile.4
  1.5 0.1 copy.12
  1.6 0.0 copy-start
  1.6 1.0 %copy-done = bf16[4,8,64,128]{3,2,1,0:T(8,128)(2,1)S(1)} copy-done((bf16[4,8,64,128]{3,2,1,0:T(8,128)(2,1)S(1)}, bf16[4,8,64,128]{3,2,1,0:T(8,128)(2,1)}, u32[]{:S(2)}) %copy-start) | copy-done | bytes 524312
  2.6 0.0 copy-start.1
  2.6 1.0 %copy-done.1 = bf16[4,8,64,128]{3,2,1,0:T(8,128)(2,1)S(1)} copy-done((bf16[4,8,64,128]{3,2,1,0:T(8,128)(2,1)S(1)}, bf16[4,8,64,128]{3,2,1,0:T(8,128)(2,1)}, u32[]{:S(2)}) %copy-start.1) | copy-done | bytes 524312
  3.7 0.0 copy-start.2
  3.7 1.0 %copy-done.2 = bf16[4,8,64,128]{3,2,1,0:T(8,128)(2,1)S(1)} copy-done((bf16[4,8,64,128]{3,2,1,0:T(8,128)(2,1)S(1)}, bf16[4,8,64,128]{3,2,1,0:T(8,128)(2,1)}, u32[]{:S(2)}) %copy-start.2) | copy-done | bytes 524312
  4.7 0.0 copy-start.3
  4.7 1.0 %copy-done.3 = bf16[1024,256]{1,0:T(8,128)(2,1)S(1)} copy-done((bf16[1024,256]{1,0:T(8,128)(2,1)S(1)}, bf16[1024,256]{1,0:T(8,128)(2,1)}, u32[]{:S(2)}) %copy-start.3) | copy-done | bytes 524312
  5.8 0.0 copy-start.4
  5.8 0.8 copy-done.4
  6.6 0.0 copy-start.5
  6.6 0.7 copy-done.5
  7.3 0.0 copy-start.6
  7.3 0.7 copy-done.6
  8.0 77.9 %cell_layer.1 = bf16[256,4096]{1,0:T(8,128)(2,1)S(1)} custom-call(f32[4,24,128]{2,1,0:T(8,128)S(1)} %pad_maximum_fusion.g_hbm, bf16[4,8,64,128]{3,2,1,0:T(8,128)(2,1)S(1)} %copy-done, bf16[4,8,64,128]{3,2,1,0:T(8,128)(2,1)S(1)} %copy-done.1, bf16[4,8,64,128]{3,2,1,0:T(8,128)(2,1)S(1)} %copy-done.2, f32[4,32,128]{2,1,0:T(8,128)S(1)} %bitcast.4, ...), custom_call_target="tpu_custom_call" | custom-call | tf_op jit(solution)/shard_map/cell_layer/pallas_call | solution.py:414
  85.9 1.3 %copy.14 = bf16[4,64,4096]{2,1,0:T(8,128)(2,1)} copy(bf16[4,64,4096]{2,1,0:T(8,128)(2,1)S(1)} %bitcast.3) | data formatting | bytes 4194304
  (4 shorter events, 0.0 us)
Async XLA Ops:
  1.6 1.0 %copy-start = (bf16[4,8,64,128]{3,2,1,0:T(8,128)(2,1)S(1)}, bf16[4,8,64,128]{3,2,1,0:T(8,128)(2,1)}, u32[]{:S(2)}) copy-start(bf16[4,8,64,128]{3,2,1,0:T(8,128)(2,1)} %q_hbm.1) | copy-start | bytes 1572868
  2.6 1.0 %copy-start.1 = (bf16[4,8,64,128]{3,2,1,0:T(8,128)(2,1)S(1)}, bf16[4,8,64,128]{3,2,1,0:T(8,128)(2,1)}, u32[]{:S(2)}) copy-start(bf16[4,8,64,128]{3,2,1,0:T(8,128)(2,1)} %k_hbm.1) | copy-start | bytes 1572868
  3.7 1.0 %copy-start.2 = (bf16[4,8,64,128]{3,2,1,0:T(8,128)(2,1)S(1)}, bf16[4,8,64,128]{3,2,1,0:T(8,128)(2,1)}, u32[]{:S(2)}) copy-start(bf16[4,8,64,128]{3,2,1,0:T(8,128)(2,1)} %v_hbm.1) | copy-start | bytes 1572868
  4.7 1.0 %copy-start.3 = (bf16[1024,256]{1,0:T(8,128)(2,1)S(1)}, bf16[1024,256]{1,0:T(8,128)(2,1)}, u32[]{:S(2)}) copy-start(bf16[1024,256]{1,0:T(8,128)(2,1)} %w_hbm.1) | copy-start | bytes 1572868
  5.8 0.8 copy-start.4
  6.6 0.7 copy-start.5
  7.3 0.7 copy-start.6

commit v2 on v1

v2 whole, which is shorter than its diff:
```python
import jax
import jax.numpy as jnp
from jax import lax
from jax.experimental import pallas as pl
from jax.experimental.pallas import tpu as pltpu
from jax.sharding import PartitionSpec as P

MESH = pl.DeviceIdType.MESH
F32 = jnp.float32
BF16 = jnp.bfloat16
S, H, T, D = 4, 8, 64, 128
NX, NZ, NY = 4, 8, 8
FACTOR = D**-0.5
NEG = -1e30
G = 4
HG = H // G
CH = 4
CROWS = 1024 // CH
LAST = 3 * CH + CH // 2


def nt(a, b):
    return lax.dot_general(a, b, (((1,), (1,)), ((), ())), preferred_element_type=F32)


def rev(i):
    return i % 2 * 4 + i // 2 % 2 * 2 + i // 4


def kernel(
    i_hbm, f_hbm, q_hbm, k_hbm, v_hbm, c_hbm, n_hbm, w_hbm, level_hbm, gain_hbm, out,
    qv, kv, vv, iv, fv, cv, nv, kx, vx, ix, fx, cx, nx, level, gain, wall, a_loc, num_s, den_s, amx_s,
    wrow, esum, amax, kvs, nkv, turn, cz_send, cz_recv, t_send, t_recv, tm_send, tm_recv,
    p_send, p_recv, pm_send, pm_recv, b_send, b_recv, bm_send, bm_recv, hid,
    lsem, xs_s, xs_r, xk_s, xk_r, tz_s, tz_r, pz_s, pz_r, xo_s, xo_r,
    wy_s, wy_r, wd_s, wd_r, wo_s, wo_r,
):
    sp = lax.axis_index("sp")
    dp = lax.axis_index("dp")
    x, z = lax.rem(sp, NX), lax.div(sp, NX)
    y, c = lax.div(dp, 2), lax.rem(dp, 2)
    mine = lax.rem(z, 2) * 4 + lax.rem(lax.div(z, 2), 2) * 2 + lax.div(z, 4)

    def xdev(d):
        return {"sp": z * NX + lax.rem(x + d, NX), "dp": dp}

    def zat(p):
        return {"sp": p * NX + x, "dp": dp}

    def ydev(d):
        return {"sp": sp, "dp": lax.rem(y + d + NY, NY) * 2 + c}

    mate = {"sp": sp, "dp": y * 2 + (1 - c)}

    def remote(src, dst, ssem, rsem, dev):
        return pltpu.make_async_remote_copy(
            src_ref=src, dst_ref=dst, send_sem=ssem, recv_sem=rsem,
            device_id=dev, device_id_type=MESH,
        )

    pairs_in = [
        (i_hbm, iv), (f_hbm, fv), (k_hbm, kv), (v_hbm, vv), (w_hbm, wall.at[dp]), (c_hbm, cv), (n_hbm, nv),
        (q_hbm, qv), (k_hbm.at[x], kx.at[x]), (v_hbm.at[x], vx.at[x]), (i_hbm.at[x], ix.at[x]),
        (f_hbm.at[x], fx.at[x]), (c_hbm.at[x], cx.at[x]), (n_hbm.at[x], nx.at[x]),
        (level_hbm, level), (gain_hbm, gain),
    ]
    loads = [pltpu.make_async_copy(src, dst, lsem.at[i]) for i, (src, dst) in enumerate(pairs_in)]
    for load in loads:
        load.start()

    barrier = pltpu.get_barrier_semaphore()
    peers = [xdev(d) for d in range(1, NX)] + [zat(lax.rem(z + d, NZ)) for d in range(1, NZ)]
    peers += [ydev(1), ydev(-1), mate]
    for dev in peers:
        pl.semaphore_signal(barrier, inc=1, device_id=dev, device_id_type=MESH)

    rows64 = lax.broadcasted_iota(jnp.int32, (T, T), 0)
    cols64 = lax.broadcasted_iota(jnp.int32, (T, T), 1)
    upper = jnp.where(rows64 <= cols64, 1.0, 0.0).astype(F32)
    causal = rows64 >= cols64

    def gates(li, f):
        li, f = li.astype(F32), f.astype(F32)
        lf = jnp.minimum(f, 0.0) - jnp.log1p(jnp.exp(-jnp.abs(f)))
        b = jnp.dot(lf, upper, precision=lax.Precision.HIGHEST, preferred_element_type=F32)
        return li - b, b[:, T - 1 : T]

    with jax.named_scope("loads"):
        for load in loads:
            load.wait()
    for j in range(S):
        a, _ = gates(iv[j], fv[j])
        a_loc[8 * j : 8 * j + 8, :] = a

    def block_gates(p):
        a, e = gates(ix[p], fx[p])
        am = jnp.max(a, axis=1, keepdims=True)
        esum[p] = jnp.broadcast_to(e, (H, D))
        amax[p] = jnp.broadcast_to(am, (H, D))
        wrow[p] = jnp.exp(a - am)

    block_gates(x)

    with jax.named_scope("barrier"):
        pl.semaphore_wait(barrier, len(peers))

    def wpart(by, bc, part):
        return wall.at[by * 2 + bc, pl.ds(part * CROWS, CROWS), :]

    def part_of(side, n):
        return (n + side * CH // 2) % CH

    def wchunk(side, n):
        by = lax.rem(y - 1 - n // CH + 2 * NY, NY) if side == 0 else lax.rem(y + 1 + n // CH, NY)
        return wpart(by, c, part_of(side, n))

    def wsend(side, n):
        if n < CH:
            ref = wpart(y, c, part_of(side, n))
        else:
            ref = wchunk(side, n - CH)
        return remote(ref, ref, wy_s.at[side, n], wy_r.at[side, n], ydev(1 if side == 0 else -1))

    def serve(n):
        for side in (0, 1):
            ref = wchunk(side, n)
            with jax.named_scope(f"serve{n}"):
                remote(ref, ref, wy_s.at[side, n], wy_r.at[side, n], ydev(1)).wait_recv()
            if n + CH < LAST:
                wsend(side, n + CH).start()
            remote(ref, ref, wd_s.at[side, n], wd_r.at[side, n], mate).start()

    def xsmall(d, here):
        p = lax.rem(x + d, NX)
        slot = x if here else lax.rem(x - d + NX, NX)
        return [
            remote(src.at[p], dst.at[slot], xs_s.at[k, d - 1], xs_r.at[k, d - 1], xdev(d))
            for k, (src, dst) in enumerate([(iv, ix), (fv, fx), (cv, cx), (nv, nx)])
        ]

    def xkeys(d, g, here):
        p = lax.rem(x + d, NX)
        slot = x if here else lax.rem(x - d + NX, NX)
        heads = pl.ds(g * HG, HG)
        return [
            remote(
                src.at[p, heads], dst.at[slot, heads],
                xk_s.at[k, g, d - 1], xk_r.at[k, g, d - 1], xdev(d),
            )
            for k, (src, dst) in enumerate([(kv, kx), (vv, vx)])
        ]

    for d in (2, 1, 3):
        for copy in xsmall(d, True)[:2]:
            copy.start()
    for g in range(G):
        for d in (2, 1, 3):
            for copy in xkeys(d, g, True):
                copy.start()
        if g == 0:
            for d in (2, 1, 3):
                for copy in xsmall(d, True)[2:]:
                    copy.start()
    for n in range(CH):
        wsend(0, n).start()
        wsend(1, n).start()
    w_own = remote(wall.at[dp], wall.at[dp], wo_s.at[0], wo_r.at[0], mate)
    w_own.start()

    def intra(i):
        j, h = lax.div(i, H), lax.rem(i, H)
        arow = a_loc[pl.ds(i, 1), :]
        masked = jnp.where(causal, jnp.broadcast_to(arow, (T, T)), NEG)
        top = jnp.max(masked, axis=1, keepdims=True)
        weight = jnp.exp(masked - top)
        scores = nt(qv[j, h], kv[j, h]) * FACTOR * weight
        den_s[i] = jnp.broadcast_to(jnp.sum(scores, axis=1, keepdims=True), (T, D))
        amx_s[i] = jnp.broadcast_to(top, (T, D))
        num_s[i] = jnp.dot(scores.astype(BF16), vv[j, h], preferred_element_type=F32)

    def inner(part):
        def body(i, _):
            for u in range(4):
                intra(part * 8 + i * 4 + u)
            return 0

        with jax.named_scope("intra"):
            lax.fori_loop(0, 2, body, 0)

    def state(p, h):
        w = wrow[p, pl.ds(h, 1), :]
        vt = vx[p, h].astype(F32).T
        hi = w.astype(BF16)
        lo = (w - hi.astype(F32)).astype(BF16)
        rid = lax.broadcasted_iota(jnp.int32, (16, T), 0)
        extra = jnp.where(
            rid == 0,
            jnp.broadcast_to(hi.astype(F32), (16, T)),
            jnp.where(rid == 1, jnp.broadcast_to(lo.astype(F32), (16, T)), 0.0),
        )
        lhs = jnp.concatenate([(vt * w).astype(BF16), extra.astype(BF16)], axis=0)
        st = jnp.dot(lhs, kx[p, h], preferred_element_type=F32)
        kvs[p, h] = st[0:D]
        nkv[p, pl.ds(h, 1), :] = st[D : D + 1] + st[D + 1 : D + 2]

    def states(p, g):
        with jax.named_scope("states"):
            for u in range(HG):
                state(p, g * HG + u)

    inner(0)

    def own(i, _):
        for u in range(4):
            state(x, i * 4 + u)
        return 0

    lax.fori_loop(0, 2, own, 0)
    inner(1)
    with jax.named_scope("xgates"):
        for d in (1, 3, 2):
            for copy in xsmall(d, False)[:2]:
                copy.wait_recv()
            block_gates(lax.rem(x - d + NX, NX))

    shift = []
    before = jnp.zeros((H, D), F32)
    top = None
    for i in range(NX):
        a = amax[i] - before
        shift.append(a)
        top = a if top is None else jnp.maximum(top, a)
        before = before + esum[i]
    scale = [jnp.exp(a - top) for a in shift]

    def tz(h):
        p = rev(h)
        d = lax.rem(p - z + NZ, NZ)
        return d, [
            remote(tm_send.at[h], tm_recv.at[z], tz_s.at[0, d], tz_r.at[0, d], zat(p)),
            remote(t_send.at[h], t_recv.at[z], tz_s.at[1, d], tz_r.at[1, d], zat(p)),
        ]

    def total(g):
        for d in (1, 3, 2):
            with jax.named_scope(f"xin{g}{d}"):
                for copy in xkeys(d, g, False):
                    copy.wait_recv()
            states(lax.rem(x - d + NX, NX), g)
        for h in range(g * HG, g * HG + HG):
            ntot = sum(scale[i][h : h + 1] * nkv[i, h : h + 1, :] for i in range(NX))
            t_send[h] = sum(scale[i][h : h + 1] * kvs[i, h] for i in range(NX)).astype(BF16)
            tm_send[h, 0:1, :] = ntot
            tm_send[h, 1:2, :] = before[h : h + 1]
            tm_send[h, 2:3, :] = top[h : h + 1]
            tm_send[h, 3:4, :] = nfirst[h : h + 1]
        for h in range(g * HG, g * HG + HG):
            d, copies = tz(h)

            @pl.when(d != 0)
            def _():
                for copy in copies:
                    copy.start()

    def cz(d):
        p = lax.rem(z + d, NZ)
        h = lax.rem(p, 2) * 4 + lax.rem(lax.div(p, 2), 2) * 2 + lax.div(p, 4)
        return remote(cz_send.at[h], cz_recv.at[z], tz_s.at[2, d], tz_r.at[2, d], zat(p))

    with jax.named_scope("xstart"):
        for d in (1, 3, 2):
            for copy in xsmall(d, False)[2:]:
                copy.wait_recv()
    for i in range(NX):
        turn[4 * i : 4 * i + 4, 0:H] = nx[i]
        for h in range(H):
            cz_send[h, 4 * i : 4 * i + 4, :] = cx[i, 4 * h : 4 * h + 4, :]
    first_lanes = lax.broadcasted_iota(jnp.int32, (H, D), 1) < 4 * NX
    nfirst = jnp.where(first_lanes, turn[...].T[0:H], 0.0)
    for d in (4, 3, 5, 2, 6, 1, 7):
        cz(d).start()

    def pz(d):
        p = lax.rem(z + d, NZ)
        return [
            remote(pm_send.at[p], pm_recv.at[mine], pz_s.at[0, d], pz_r.at[0, d], zat(p)),
            remote(p_send.at[p], p_recv.at[mine], pz_s.at[1, d], pz_r.at[1, d], zat(p)),
        ]

    def scan(g):
        @pl.when(lax.div(mine, HG) == g)
        def _():
            with jax.named_scope(f"zin{g}"):
                for d in range(1, NZ):
                    p = lax.rem(z - d + NZ, NZ)
                    for src, dst, k in ((tm_send, tm_recv, 0), (t_send, t_recv, 1), (cz_send, cz_recv, 2)):
                        remote(src.at[0], dst.at[p], tz_s.at[k, d], tz_r.at[k, d], zat(p)).wait_recv()
            with jax.named_scope("scan"):
                t_recv[z] = t_send[mine]
                tm_recv[z] = tm_send[mine]
                cz_recv[z] = cz_send[mine]
                lanes = lax.broadcasted_iota(jnp.int32, (1, H), 1)
                m = jnp.sum(jnp.where(lanes == mine, level[pl.ds(x, 1), :], 0.0), axis=1, keepdims=True)
                m = jnp.broadcast_to(m, (1, D))
                nrow = tm_recv[0, 3:4, :]
                for i in range(1, NZ):
                    nrow = nrow + pltpu.roll(tm_recv[i, 3:4, :], 4 * NX * i, 1)
                cur = jnp.concatenate([cz_recv[i] for i in range(NZ)], axis=0).T
                for i in range(NZ):
                    p_send[i] = cur.astype(BF16)
                    pm_send[i, 0:1, :] = nrow
                    pm_send[i, 1:2, :] = m
                    am = tm_recv[i, 2:3, :]
                    hi = jnp.maximum(m, am)
                    keep, add = jnp.exp(m - hi), jnp.exp(am - hi)
                    cur = keep * cur + add * t_recv[i].astype(F32)
                    nrow = keep * nrow + add * tm_recv[i, 0:1, :]
                    m = tm_recv[i, 1:2, :] + hi
                for d in (4, 3, 5, 2, 6, 1, 7):
                    for copy in pz(d):
                        copy.start()
                p_recv[mine] = p_send[z]
                pm_recv[mine] = pm_send[z]

    def xo(d, g, here):
        p = lax.rem(x + d, NX)
        slot = x if here else lax.rem(x - d + NX, NX)
        heads = pl.ds(g * HG, HG)
        return [
            remote(
                bm_send.at[p, g], bm_recv.at[slot, g],
                xo_s.at[0, g, d - 1], xo_r.at[0, g, d - 1], xdev(d),
            ),
            remote(
                b_send.at[p, heads], b_recv.at[slot, heads],
                xo_s.at[1, g, d - 1], xo_r.at[1, g, d - 1], xdev(d),
            ),
        ]

    def spread(g):
        for h in range(g * HG, g * HG + HG):
            p = rev(h)
            d = lax.rem(z - p + NZ, NZ)

            @pl.when(d != 0)
            def _():
                with jax.named_scope(f"zout{g}"):
                    for src, dst, k in ((pm_send, pm_recv, 0), (p_send, p_recv, 1)):
                        remote(src.at[0], dst.at[h], pz_s.at[k, d], pz_r.at[k, d], zat(p)).wait_recv()

        for u in range(HG):
            h = g * HG + u
            cur = p_recv[h].astype(F32)
            nrow = pm_recv[h, 0:1, :]
            m = pm_recv[h, 1:2, :]
            for i in range(NX):
                b_send[i, h] = cur.astype(BF16)
                bm_send[i, g, 2 * u : 2 * u + 1, :] = nrow
                bm_send[i, g, 2 * u + 1 : 2 * u + 2, :] = m
                if i < NX - 1:
                    am = amax[i, h : h + 1, :]
                    hi = jnp.maximum(m, am)
                    keep, add = jnp.exp(m - hi), jnp.exp(am - hi)
                    cur = keep * cur + add * kvs[i, h]
                    nrow = keep * nrow + add * nkv[i, h : h + 1, :]
                    m = esum[i, h : h + 1, :] + hi
        for d in (2, 1, 3):
            for copy in xo(d, g, True):
                copy.start()
        heads = pl.ds(g * HG, HG)
        b_recv[x, heads] = b_send[x, heads]
        bm_recv[x, g] = bm_send[x, g]

    def finish_one(j, g):
        for u in range(HG):
            h = g * HG + u
            i = j * H + h
            q = qv[j, h]
            nrow = bm_recv[j, g, 2 * u : 2 * u + 1, :]
            m = bm_recv[j, g, 2 * u + 1 : 2 * u + 2, :]
            qc = nt(q, b_recv[j, h])
            qn = jnp.sum(q.astype(F32) * nrow, axis=1, keepdims=True)
            a = amx_s[i]
            hi = jnp.maximum(a, m)
            keep, add = jnp.exp(m - hi) * FACTOR, jnp.exp(a - hi)
            den = add * den_s[i] + keep * qn
            num = add * num_s[i] + keep * qc
            o = (num / jnp.maximum(jnp.abs(den), 1.0)).astype(BF16)
            normed = (o.astype(F32) * gain[h : h + 1, :]).astype(BF16)
            hid[pl.ds(pl.multiple_of(j * T, T), T), h * D : h * D + D] = normed

    def finish(g):
        with jax.named_scope("finish"):
            finish_one(x, g)
        for d in (1, 3, 2):
            with jax.named_scope(f"xout{g}{d}"):
                for copy in xo(d, g, False):
                    copy.wait_recv()
            with jax.named_scope("finish"):
                finish_one(lax.rem(x - d + NX, NX), g)

    def project(dist):
        def body(i, _):
            t = lax.div(i, 2)
            away = lax.div(t + 1, 2) * (1 - 2 * lax.rem(t, 2))
            block = lax.rem(y + away + NY, NY) * 2 + lax.rem(i, 2)
            cols = pl.ds(pl.multiple_of(block * 256, 256), 256)
            out[:, cols] = jnp.dot(hid[...], wall[block], preferred_element_type=F32).astype(BF16)
            return 0

        if dist == 0:
            low, high = 0, 2
            remote(wall.at[dp], wall.at[y * 2 + 1 - c], wo_s.at[0], wo_r.at[0], mate).wait_recv()
        else:
            low, high = 4 * dist - 2, min(4 * dist + 2, 4 * NY // 2)
            with jax.named_scope(f"mate{dist}"):
                for n in range(CH * dist - CH, min(CH * dist, LAST)):
                    for side in (0, 1):
                        ref = wchunk(side, n)
                        remote(ref, ref, wd_s.at[side, n], wd_r.at[side, n], mate).wait_recv()
        with jax.named_scope("project"):
            lax.fori_loop(low, high, body, 0)

    total(0)
    serve(0)
    inner(2)
    total(1)
    serve(1)
    inner(3)
    scan(0)
    total(2)
    serve(2)
    scan(1)
    serve(3)
    total(3)
    spread(0)
    scan(2)
    serve(4)
    spread(1)
    scan(3)
    serve(5)
    finish(0)
    spread(2)
    serve(6)
    finish(1)
    spread(3)
    serve(7)
    finish(2)
    serve(8)
    finish(3)
    project(0)
    project(1)
    serve(9)
    project(2)
    serve(10)
    serve(11)
    project(3)
    serve(12)
    serve(13)
    project(4)

    for d in range(1, NX):
        for copy in xsmall(d, True):
            copy.wait_send()
        for g in range(G):
            for copy in xkeys(d, g, True) + xo(d, g, True):
                copy.wait_send()
    for d in range(1, NZ):
        p = lax.rem(z + d, NZ)
        for src, dst, k in ((tm_send, tm_recv, 0), (t_send, t_recv, 1), (cz_send, cz_recv, 2)):
            remote(src.at[0], dst.at[0], tz_s.at[k, d], tz_r.at[k, d], zat(p)).wait_send()
        for copy in pz(d):
            copy.wait_send()
    w_own.wait_send()
    for n in range(LAST):
        for side in (0, 1):
            wsend(side, n).wait_send()
            ref = wchunk(side, n)
            remote(ref, ref, wd_s.at[side, n], wd_r.at[side, n], mate).wait_send()


def on_device(queries, keys, values, input_gate, forget_gate, start_memory, start_norm, start_level, head_gain, out_weight):
    arrays = (
        input_gate, forget_gate, queries, keys, values, start_memory.reshape(S, 32, D),
        jnp.transpose(start_norm, (0, 2, 1)), out_weight, start_level, head_gain,
    )
    dma, vmem = pltpu.SemaphoreType.DMA, pltpu.VMEM
    out = pl.pallas_call(
        kernel,
        out_shape=pltpu.VMEM((S * T, 4096), BF16),
        in_specs=[pl.BlockSpec(memory_space=pltpu.HBM)] * len(arrays),
        out_specs=pl.BlockSpec(memory_space=pltpu.VMEM),
        scratch_shapes=[
            vmem((S, H, T, D), BF16), vmem((S, H, T, D), BF16), vmem((S, H, T, D), BF16),
            vmem((S, H, T), BF16), vmem((S, H, T), BF16), vmem((S, 32, D), F32), vmem((S, 4, H), F32),
            vmem((NX, H, T, D), BF16), vmem((NX, H, T, D), BF16),
            vmem((NX, H, T), BF16), vmem((NX, H, T), BF16), vmem((NX, 32, D), F32), vmem((NX, 4, H), F32),
            vmem((S, H), F32), vmem((H, D), F32),
            vmem((2 * NY, 1024, 256), BF16),
            vmem((S * H, T), F32),
            vmem((S * H, T, D), F32), vmem((S * H, T, D), F32), vmem((S * H, T, D), F32),
            vmem((NX, H, T), F32), vmem((NX, H, D), F32), vmem((NX, H, D), F32),
            vmem((NX, H, D, D), F32), vmem((NX, H, D), F32), vmem((D, D), F32),
            vmem((H, 16, D), F32), vmem((NZ, 16, D), F32),
            vmem((H, D, D), BF16), vmem((NZ, D, D), BF16),
            vmem((H, 8, D), F32), vmem((NZ, 8, D), F32),
            vmem((NZ, D, D), BF16), vmem((H, D, D), BF16),
            vmem((NZ, 8, D), F32), vmem((H, 8, D), F32),
            vmem((NX, H, D, D), BF16), vmem((S, H, D, D), BF16),
            vmem((NX, G, 8, D), F32), vmem((S, G, 8, D), F32),
            vmem((S * T, H * D), BF16),
            dma((16,)),
            dma((4, 3)), dma((4, 3)), dma((2, G, 3)), dma((2, G, 3)),
            dma((3, 8)), dma((3, 8)), dma((2, 8)), dma((2, 8)),
            dma((2, G, 3)), dma((2, G, 3)),
            dma((2, LAST)), dma((2, LAST)), dma((2, LAST)), dma((2, LAST)),
            dma((1,)), dma((1,)),
        ],
        compiler_params=pltpu.CompilerParams(
            collective_id=0, has_side_effects=True, vmem_limit_bytes=50_000_000
        ),
        name="cell_layer",
    )(*(pltpu.with_memory_space_constraint(array, pltpu.HBM) for array in arrays))
    return out.reshape(S, T, 4096)


def solution(mesh):
    return jax.shard_map(
        on_device,
        mesh=mesh,
        in_specs=(
            P("dp", None, "sp", None),
            P("dp", None, "sp", None),
            P("dp", None, "sp", None),
            P("dp", None, "sp"),
            P("dp", None, "sp"),
            P("dp", None, "sp", None),
            P("dp", None, "sp"),
            P("dp", None),
            P(),
            P(None, "dp"),
        ),
        out_specs=P("dp", "sp", None),
        check_vma=False,
    )
```

time: 87.7 us -> 63.1 us (0.72)
  Pallas kernels: 77.9 us -> 61.6 us
  local copies, waits for them, and re-layouts: 8.51 us -> 1.32 us
    pallas_call x1, Pallas kernels: 77.9 us -> 61.6 us  [on_device(): pl.pallas_call(kernel, out_shape=pltpu.VMEM((S * T, 4096), BF16), in_spec...]
    unnamed x15 -> x1, local copies, waits for them, and re-layouts: 7.69 us -> 1.32 us
where the time goes in v2:
time: 63.1 us; the launch traced here: 63 us
  Pallas kernels  61.6 us (98%)
  local copies, waits for them, and re-layouts  1.32 us (2%)
    pallas_call x1, Pallas kernels, on_device(): pl.pallas_call(kernel, out_shape=pltpu.VMEM((S * T, 4096), BF16), in_spec...  61.6 us
    unnamed x1, local copies, waits for them, and re-layouts  1.32 us

profile of v2, /device:TPU:1, one launch (start us, length us, event | category | flops | bytes accessed | tf_op | source)
XLA Modules:
  0.0 63.0 jit_solution(8950986019215413845)
XLA Ops:
  0.0 61.6 %cell_layer.1 = bf16[256,4096]{1,0:T(8,128)(2,1)S(1)} custom-call(bf16[4,8,64]{2,1,0:T(8,128)(2,1)} %i_hbm.1, bf16[4,8,64]{2,1,0:T(8,128)(2,1)} %f_hbm.1, bf16[4,8,64,128]{3,2,1,0:T(8,128)(2,1)} %q_hbm.1, bf16[4,8,64,128]{3,2,1,0:T(8,128)(2,1)} %k_hbm.1, bf16[4,8,64,128]{3,2,1,0:T(8,128)(2,1)} %v_hbm.1, f32[4,32,128]{2,1,0:T(8,128)} %bitcast.4, ...), custom_call_target="tpu_custom_call" | custom-call | tf_op jit(solution)/shard_map/cell_layer/pallas_call | solution.py:488
  61.6 1.3 %copy.12 = bf16[4,64,4096]{2,1,0:T(8,128)(2,1)} copy(bf16[4,64,4096]{2,1,0:T(8,128)(2,1)S(1)} %bitcast.3) | data formatting | bytes 4194304

commit v3 on v2

--- a/solution.py
+++ b/solution.py
@@ -14,9 +14,8 @@
 NEG = -1e30
 G = 4
 HG = H // G
-CH = 4
-CROWS = 1024 // CH
-LAST = 3 * CH + CH // 2
+RA = 768
+RB = (1024 - RA) // NX
 
 
 def nt(a, b):
@@ -31,9 +30,9 @@
     i_hbm, f_hbm, q_hbm, k_hbm, v_hbm, c_hbm, n_hbm, w_hbm, level_hbm, gain_hbm, out,
     qv, kv, vv, iv, fv, cv, nv, kx, vx, ix, fx, cx, nx, level, gain, wall, a_loc, num_s, den_s, amx_s,
     wrow, esum, amax, kvs, nkv, turn, cz_send, cz_recv, t_send, t_recv, tm_send, tm_recv,
-    p_send, p_recv, pm_send, pm_recv, b_send, b_recv, bm_send, bm_recv, hid,
+    p_send, p_recv, pm_send, pm_recv, b_send, b_recv, bm_send, bm_recv, hid, acc,
     lsem, xs_s, xs_r, xk_s, xk_r, tz_s, tz_r, pz_s, pz_r, xo_s, xo_r,
-    wy_s, wy_r, wd_s, wd_r, wo_s, wo_r,
+    wy_s, wy_r, wd_s, wd_r, wo_s, wo_r, ws_s, ws_r,
 ):
     sp = lax.axis_index("sp")
     dp = lax.axis_index("dp")
@@ -58,8 +57,14 @@
             device_id=dev, device_id_type=MESH,
         )
 
+    barrier = pltpu.get_barrier_semaphore()
+    peers = [xdev(d) for d in range(1, NX)] + [zat(lax.rem(z + d, NZ)) for d in range(1, NZ)]
+    peers += [ydev(1), ydev(-1), mate]
+    for dev in peers:
+        pl.semaphore_signal(barrier, inc=1, device_id=dev, device_id_type=MESH)
+
     pairs_in = [
-        (i_hbm, iv), (f_hbm, fv), (k_hbm, kv), (v_hbm, vv), (w_hbm, wall.at[dp]), (c_hbm, cv), (n_hbm, nv),
+        (i_hbm, iv), (f_hbm, fv), (k_hbm, kv), (v_hbm, vv), (w_hbm, wall.at[c, 0]), (c_hbm, cv), (n_hbm, nv),
         (q_hbm, qv), (k_hbm.at[x], kx.at[x]), (v_hbm.at[x], vx.at[x]), (i_hbm.at[x], ix.at[x]),
         (f_hbm.at[x], fx.at[x]), (c_hbm.at[x], cx.at[x]), (n_hbm.at[x], nx.at[x]),
         (level_hbm, level), (gain_hbm, gain),
@@ -68,12 +73,6 @@
     for load in loads:
         load.start()
 
-    barrier = pltpu.get_barrier_semaphore()
-    peers = [xdev(d) for d in range(1, NX)] + [zat(lax.rem(z + d, NZ)) for d in range(1, NZ)]
-    peers += [ydev(1), ydev(-1), mate]
-    for dev in peers:
-        pl.semaphore_signal(barrier, inc=1, device_id=dev, device_id_type=MESH)
-
     rows64 = lax.broadcasted_iota(jnp.int32, (T, T), 0)
     cols64 = lax.broadcasted_iota(jnp.int32, (T, T), 1)
     upper = jnp.where(rows64 <= cols64, 1.0, 0.0).astype(F32)
@@ -104,31 +103,84 @@
     with jax.named_scope("barrier"):
         pl.semaphore_wait(barrier, len(peers))
 
-    def wpart(by, bc, part):
-        return wall.at[by * 2 + bc, pl.ds(part * CROWS, CROWS), :]
-
-    def part_of(side, n):
-        return (n + side * CH // 2) % CH
-
-    def wchunk(side, n):
-        by = lax.rem(y - 1 - n // CH + 2 * NY, NY) if side == 0 else lax.rem(y + 1 + n // CH, NY)
-        return wpart(by, c, part_of(side, n))
-
-    def wsend(side, n):
-        if n < CH:
-            ref = wpart(y, c, part_of(side, n))
+    def rows_of(side, kind):
+        if kind == "b":
+            return pl.ds(pl.multiple_of(RA + RB * x, RB), RB)
+        if kind == "half":
+            return pl.ds(pl.multiple_of(RA + RB * x + side * (RB // 2), RB // 2), RB // 2)
+        if kind == "cut":
+            return pl.ds(256 + 128 * side, 128)
+        return pl.ds(256 * (2 - kind if side else kind), 256)
+
+    ring = [(0, "b"), (0, 0), (1, "b"), (0, 1), (2, "b"), (0, 2), (3, "half")]
+    ring += [(1, 0), (1, 1), (1, 2), (2, 0), (2, 1), (2, 2), (3, 0), (3, "cut")]
+    onward = {(0, "b"): (1, "b"), (1, "b"): (2, "b"), (2, "b"): (3, "half"), (2, 1): (3, "cut")}
+    for k in range(3):
+        onward[0, k], onward[1, k] = (1, k), (2, k)
+    onward[2, 0] = (3, 0)
+
+    def wsend(side, item):
+        level, kind = item
+        k = ring.index(item)
+        rows = rows_of(side, kind)
+        src, dst = (level, level + 1) if side else ((NY - level) % NY, NY - 1 - level)
+        return remote(
+            wall.at[c, src, rows], wall.at[c, dst, rows],
+            wy_s.at[side, k], wy_r.at[side, k], ydev(-1 if side else 1),
+        )
+
+    def wmate(side, item):
+        level, kind = item
+        k = ring.index(item)
+        ref = wall.at[c, level + 1 if side else NY - 1 - level, rows_of(side, kind)]
+        return remote(ref, ref, wd_s.at[side, k], wd_r.at[side, k], mate)
+
+    def wmate_recv(side, item):
+        level, kind = item
+        k = ring.index(item)
+        ref = wall.at[1 - c, level + 1 if side else NY - 1 - level, rows_of(side, kind)]
+        return remote(ref, ref, wd_s.at[side, k], wd_r.at[side, k], mate)
+
+    def serve(level, kind):
+        item = (level, kind)
+        with jax.named_scope(f"serve{level}{kind}"):
+            for side in (0, 1):
+                wsend(side, item).wait_recv()
+        for side in (0, 1):
+            if item in onward:
+                wsend(side, onward[item]).start()
+            if kind not in ("b", "half"):
+                wmate(side, item).start()
+
+    def begin(level, kind):
+        for side in (0, 1):
+            wsend(side, (level, kind)).start()
+
+    def wspread(k):
+        side, far = k % 2, k // 2
+        to = xdev(NX - 1 if side else 1)
+        if far:
+            own = lax.rem(x + (1 if side else NX - 1), NX)
+            rows = pl.ds(pl.multiple_of(RA + RB * own + side * (RB // 2), RB // 2), RB // 2)
         else:
-            ref = wchunk(side, n - CH)
-        return remote(ref, ref, wy_s.at[side, n], wy_r.at[side, n], ydev(1 if side == 0 else -1))
-
-    def serve(n):
-        for side in (0, 1):
-            ref = wchunk(side, n)
-            with jax.named_scope(f"serve{n}"):
-                remote(ref, ref, wy_s.at[side, n], wy_r.at[side, n], ydev(1)).wait_recv()
-            if n + CH < LAST:
-                wsend(side, n + CH).start()
-            remote(ref, ref, wd_s.at[side, n], wd_r.at[side, n], mate).start()
+            rows = pl.ds(pl.multiple_of(RA + RB * x, RB), RB)
+        ref = wall.at[c, 1:NY, rows]
+        return remote(ref, ref, ws_s.at[k], ws_r.at[k], to)
+
+    def wspread_recv(k):
+        side, far = k % 2, k // 2
+        away = (2 if far else 1) if side else NX - (2 if far else 1)
+        own = lax.rem(x + away, NX)
+        if far:
+            rows = pl.ds(pl.multiple_of(RA + RB * own + side * (RB // 2), RB // 2), RB // 2)
+        else:
+            rows = pl.ds(pl.multiple_of(RA + RB * own, RB), RB)
+        ref = wall.at[c, 1:NY, rows]
+        return remote(ref, ref, ws_s.at[k], ws_r.at[k], xdev(1))
+
+    def wrest(core):
+        ref = wall.at[core, 1:NY, RA:1024]
+        return remote(ref, ref, ws_s.at[4], ws_r.at[4], mate)
 
     def xsmall(d, here):
         p = lax.rem(x + d, NX)
@@ -150,21 +202,17 @@
             for k, (src, dst) in enumerate([(kv, kx), (vv, vx)])
         ]
 
+    begin(0, "b")
+    begin(0, 0)
     for d in (2, 1, 3):
-        for copy in xsmall(d, True)[:2]:
+        for copy in xsmall(d, True):
             copy.start()
     for g in range(G):
         for d in (2, 1, 3):
             for copy in xkeys(d, g, True):
                 copy.start()
-        if g == 0:
-            for d in (2, 1, 3):
-                for copy in xsmall(d, True)[2:]:
-                    copy.start()
-    for n in range(CH):
-        wsend(0, n).start()
-        wsend(1, n).start()
-    w_own = remote(wall.at[dp], wall.at[dp], wo_s.at[0], wo_r.at[0], mate)
+    ref = wall.at[c, 0]
+    w_own = remote(ref, ref, wo_s.at[0], wo_r.at[0], mate)
     w_own.start()
 
     def intra(i):
@@ -216,10 +264,11 @@
         return 0
 
     lax.fori_loop(0, 2, own, 0)
-    inner(1)
+    serve(0, "b")
+    begin(0, 1)
     with jax.named_scope("xgates"):
         for d in (1, 3, 2):
-            for copy in xsmall(d, False)[:2]:
+            for copy in xsmall(d, False):
                 copy.wait_recv()
             block_gates(lax.rem(x - d + NX, NX))
 
@@ -267,18 +316,12 @@
         h = lax.rem(p, 2) * 4 + lax.rem(lax.div(p, 2), 2) * 2 + lax.div(p, 4)
         return remote(cz_send.at[h], cz_recv.at[z], tz_s.at[2, d], tz_r.at[2, d], zat(p))
 
-    with jax.named_scope("xstart"):
-        for d in (1, 3, 2):
-            for copy in xsmall(d, False)[2:]:
-                copy.wait_recv()
     for i in range(NX):
         turn[4 * i : 4 * i + 4, 0:H] = nx[i]
         for h in range(H):
             cz_send[h, 4 * i : 4 * i + 4, :] = cx[i, 4 * h : 4 * h + 4, :]
     first_lanes = lax.broadcasted_iota(jnp.int32, (H, D), 1) < 4 * NX
     nfirst = jnp.where(first_lanes, turn[...].T[0:H], 0.0)
-    for d in (4, 3, 5, 2, 6, 1, 7):
-        cz(d).start()
 
     def pz(d):
         p = lax.rem(z + d, NZ)
@@ -399,84 +442,143 @@
             with jax.named_scope("finish"):
                 finish_one(lax.rem(x - d + NX, NX), g)
 
-    def project(dist):
+    def columns(core, r):
+        block = lax.rem(y + r, NY) * 2 + core
+        return pl.ds(pl.multiple_of(block * 256, 256), 256)
+
+    def early(slots):
         def body(i, _):
-            t = lax.div(i, 2)
-            away = lax.div(t + 1, 2) * (1 - 2 * lax.rem(t, 2))
-            block = lax.rem(y + away + NY, NY) * 2 + lax.rem(i, 2)
-            cols = pl.ds(pl.multiple_of(block * 256, 256), 256)
-            out[:, cols] = jnp.dot(hid[...], wall[block], preferred_element_type=F32).astype(BF16)
+            core = lax.rem(i, 2)
+            r = lax.rem(slots[0] + lax.div(i, 2), NY)
+            acc[core, r] = jnp.dot(hid[:, 0:RA], wall[core, r, 0:RA], preferred_element_type=F32)
             return 0
 
-        if dist == 0:
-            low, high = 0, 2
-            remote(wall.at[dp], wall.at[y * 2 + 1 - c], wo_s.at[0], wo_r.at[0], mate).wait_recv()
-        else:
-            low, high = 4 * dist - 2, min(4 * dist + 2, 4 * NY // 2)
-            with jax.named_scope(f"mate{dist}"):
-                for n in range(CH * dist - CH, min(CH * dist, LAST)):
-                    for side in (0, 1):
-                        ref = wchunk(side, n)
-                        remote(ref, ref, wd_s.at[side, n], wd_r.at[side, n], mate).wait_recv()
-        with jax.named_scope("project"):
-            lax.fori_loop(low, high, body, 0)
-
+        with jax.named_scope("early"):
+            lax.fori_loop(0, 2 * len(slots), body, 0)
+
+    def mates(items):
+        with jax.named_scope("mate"):
+            for item in items:
+                for side in (0, 1):
+                    wmate_recv(side, item).wait_recv()
+
+    def late():
+        def body(i, _):
+            core = lax.rem(i, 2)
+            r = lax.rem(NY - 3 + lax.div(i, 2), NY)
+            part = jnp.dot(hid[:, RA:1024], wall[core, r, RA:1024], preferred_element_type=F32)
+            out[:, columns(core, r)] = (acc[core, r] + part).astype(BF16)
+            return 0
+
+        with jax.named_scope("late"):
+            lax.fori_loop(0, 2 * (NY - 1), body, 0)
+
+    def last():
+        def body(core, _):
+            whole = jnp.dot(hid[...], wall[core, NY // 2], preferred_element_type=F32)
+            out[:, columns(core, NY // 2)] = whole.astype(BF16)
+            return 0
+
+        with jax.named_scope("last"):
+            lax.fori_loop(0, 2, body, 0)
+
+    def sent_w(*items):
+        for item in items:
+            for side in (0, 1):
+                wsend(side, item).wait_send()
+
+    def sent_mate(*items):
+        for item in items:
+            for side in (0, 1):
+                wmate(side, item).wait_send()
+
+    for d in (4, 3, 5, 2, 6, 1, 7):
+        cz(d).start()
+    inner(1)
     total(0)
-    serve(0)
+    serve(1, "b")
+    begin(0, 2)
     inner(2)
     total(1)
-    serve(1)
+    serve(2, "b")
+    serve(0, 0)
+    serve(0, 1)
     inner(3)
+    total(2)
+    serve(3, "half")
+    wspread(0).start()
+    wspread(1).start()
     scan(0)
-    total(2)
-    serve(2)
+    serve(0, 2)
+    total(3)
     scan(1)
-    serve(3)
-    total(3)
-    spread(0)
-    scan(2)
-    serve(4)
-    spread(1)
-    scan(3)
-    serve(5)
-    finish(0)
-    spread(2)
-    serve(6)
-    finish(1)
-    spread(3)
-    serve(7)
-    finish(2)
-    serve(8)
-    finish(3)
-    project(0)
-    project(1)
-    serve(9)
-    project(2)
-    serve(10)
-    serve(11)
-    project(3)
-    serve(12)
-    serve(13)
-    project(4)
-
+    serve(1, 0)
     for d in range(1, NX):
         for copy in xsmall(d, True):
             copy.wait_send()
         for g in range(G):
-            for copy in xkeys(d, g, True) + xo(d, g, True):
+            for copy in xkeys(d, g, True):
                 copy.wait_send()
+    serve(1, 1)
+    spread(0)
+    with jax.named_scope("wspread"):
+        wspread_recv(0).wait_recv()
+        wspread_recv(1).wait_recv()
+    wspread(2).start()
+    wspread(3).start()
+    scan(2)
+    spread(1)
+    serve(1, 2)
+    scan(3)
+    sent_w((0, "b"), (1, "b"), (2, "b"), (3, "half"), (0, 0), (0, 1), (0, 2))
+    finish(0)
+    serve(2, 0)
+    spread(2)
     for d in range(1, NZ):
         p = lax.rem(z + d, NZ)
         for src, dst, k in ((tm_send, tm_recv, 0), (t_send, t_recv, 1), (cz_send, cz_recv, 2)):
             remote(src.at[0], dst.at[0], tz_s.at[k, d], tz_r.at[k, d], zat(p)).wait_send()
+    finish(1)
+    serve(2, 1)
+    spread(3)
+    with jax.named_scope("wspread"):
+        wspread_recv(2).wait_recv()
+        wspread_recv(3).wait_recv()
+    wrest(c).start()
+    finish(2)
+    serve(2, 2)
+    ref = wall.at[1 - c, 0]
+    remote(ref, ref, wo_s.at[0], wo_r.at[0], mate).wait_recv()
+    mates([(0, 0), (0, 1), (0, 2), (1, 0), (1, 1), (1, 2)])
+    early([6, 7, 0, 1, 2])
+    sent_w((1, 0), (1, 1), (1, 2))
+    sent_mate((0, 0), (0, 1), (0, 2), (1, 0), (1, 1), (1, 2))
+    for d in range(1, NZ):
         for copy in pz(d):
             copy.wait_send()
+    mates([(2, 0), (2, 1), (2, 2)])
+    early([3])
+    early([5])
+    finish(3)
+    serve(3, 0)
+    with jax.named_scope("rest"):
+        wrest(1 - c).wait_recv()
+    late()
+    serve(3, "cut")
+    for d in range(1, NX):
+        for g in range(G):
+            for copy in xo(d, g, True):
+                copy.wait_send()
+    sent_w((2, 0), (2, 1), (2, 2))
+    sent_mate((2, 0), (2, 1), (2, 2))
     w_own.wait_send()
-    for n in range(LAST):
-        for side in (0, 1):
-            wsend(side, n).wait_send()
-            ref = wchunk(side, n)
-            remote(ref, ref, wd_s.at[side, n], wd_r.at[side, n], mate).wait_send()
+    for k in range(4):
+        wspread(k).wait_send()
+    wrest(c).wait_send()
+    mates([(3, 0), (3, "cut")])
+    last()
+    sent_w((3, 0), (3, "cut"))
+    sent_mate((3, 0), (3, "cut"))
 
 
 def on_device(queries, keys, values, input_gate, forget_gate, start_memory, start_norm, start_level, head_gain, out_weight):
@@ -496,7 +598,7 @@
             vmem((NX, H, T, D), BF16), vmem((NX, H, T, D), BF16),
             vmem((NX, H, T), BF16), vmem((NX, H, T), BF16), vmem((NX, 32, D), F32), vmem((NX, 4, H), F32),
             vmem((S, H), F32), vmem((H, D), F32),
-            vmem((2 * NY, 1024, 256), BF16),
+            vmem((2, NY, 1024, 256), BF16),
             vmem((S * H, T), F32),
             vmem((S * H, T, D), F32), vmem((S * H, T, D), F32), vmem((S * H, T, D), F32),
             vmem((NX, H, T), F32), vmem((NX, H, D), F32), vmem((NX, H, D), F32),
@@ -508,13 +610,13 @@
             vmem((NZ, 8, D), F32), vmem((H, 8, D), F32),
             vmem((NX, H, D, D), BF16), vmem((S, H, D, D), BF16),
             vmem((NX, G, 8, D), F32), vmem((S, G, 8, D), F32),
-            vmem((S * T, H * D), BF16),
+            vmem((S * T, H * D), BF16), vmem((2, NY, S * T, 256), F32),
             dma((16,)),
             dma((4, 3)), dma((4, 3)), dma((2, G, 3)), dma((2, G, 3)),
             dma((3, 8)), dma((3, 8)), dma((2, 8)), dma((2, 8)),
             dma((2, G, 3)), dma((2, G, 3)),
-            dma((2, LAST)), dma((2, LAST)), dma((2, LAST)), dma((2, LAST)),
-            dma((1,)), dma((1,)),
+            dma((2, 15)), dma((2, 15)), dma((2, 15)), dma((2, 15)),
+            dma((1,)), dma((1,)), dma((5,)), dma((5,)),
         ],
         compiler_params=pltpu.CompilerParams(
             collective_id=0, has_side_effects=True, vmem_limit_bytes=50_000_000

time: 63.1 us -> 62.3 us (0.987)
  Pallas kernels: 61.6 us -> 60.8 us
    pallas_call x1, Pallas kernels: 61.6 us -> 60.8 us  [on_device(): pl.pallas_call(kernel, out_shape=pltpu.VMEM((S * T, 4096), BF16), in_spec...]
where the time goes in v3:
time: 62.3 us; the launch traced here: 62.1 us
  Pallas kernels  60.8 us (98%)
  local copies, waits for them, and re-layouts  1.32 us (2%)
    pallas_call x1, Pallas kernels, on_device(): pl.pallas_call(kernel, out_shape=pltpu.VMEM((S * T, 4096), BF16), in_spec...  60.8 us
    unnamed x1, local copies, waits for them, and re-layouts  1.32 us

profile of v3, /device:TPU:1, one launch (start us, length us, event | category | flops | bytes accessed | tf_op | source)
XLA Modules:
  0.0 62.1 jit_solution(14071135197879817112)
XLA Ops:
  0.0 60.8 %cell_layer.1 = bf16[256,4096]{1,0:T(8,128)(2,1)S(1)} custom-call(bf16[4,8,64]{2,1,0:T(8,128)(2,1)} %i_hbm.1, bf16[4,8,64]{2,1,0:T(8,128)(2,1)} %f_hbm.1, bf16[4,8,64,128]{3,2,1,0:T(8,128)(2,1)} %q_hbm.1, bf16[4,8,64,128]{3,2,1,0:T(8,128)(2,1)} %k_hbm.1, bf16[4,8,64,128]{3,2,1,0:T(8,128)(2,1)} %v_hbm.1, f32[4,32,128]{2,1,0:T(8,128)} %bitcast.4, ...), custom_call_target="tpu_custom_call" | custom-call | tf_op jit(solution)/shard_map/cell_layer/pallas_call | solution.py:590
  60.8 1.3 %copy.12 = bf16[4,64,4096]{2,1,0:T(8,128)(2,1)} copy(bf16[4,64,4096]{2,1,0:T(8,128)(2,1)S(1)} %bitcast.3) | data formatting | bytes 4194304

commit v4 on v3

v4 whole, which is shorter than its diff:
```python
import jax
import jax.numpy as jnp
from jax import lax
from jax.experimental import pallas as pl
from jax.experimental.pallas import tpu as pltpu
from jax.sharding import PartitionSpec as P

MESH = pl.DeviceIdType.MESH
F32 = jnp.float32
BF16 = jnp.bfloat16
S, H, T, D = 4, 8, 64, 128
NX, NZ, NY = 4, 8, 8
FACTOR = D**-0.5
NEG = -1e30
G = 4
HG = H // G
RA = 768
RB = (1024 - RA) // NX


def nt(a, b):
    return lax.dot_general(a, b, (((1,), (1,)), ((), ())), preferred_element_type=F32)


def rev(i):
    return i % 2 * 4 + i // 2 % 2 * 2 + i // 4


def kernel(
    i_hbm, f_hbm, q_hbm, k_hbm, v_hbm, c_hbm, n_hbm, w_hbm, level_hbm, gain_hbm, out,
    qv, kv, vv, iv, fv, cv, nv, kx, vx, ix, fx, cx, nx, level, gain, wall, a_loc, num_s, den_s, amx_s,
    wrow, esum, amax, kvs, nkv, turn, cz_send, cz_recv, t_send, t_recv, tm_send, tm_recv,
    p_send, p_recv, pm_send, pm_recv, b_send, b_recv, bm_send, bm_recv, hid, acc,
    lsem, sent, xs_r, xk_r, tz_r, pz_r, xo_r, wy_r, wd_r, ws_r, wo_r, hello,
):
    sp = lax.axis_index("sp")
    dp = lax.axis_index("dp")
    x, z = lax.rem(sp, NX), lax.div(sp, NX)
    y, c = lax.div(dp, 2), lax.rem(dp, 2)
    mine = lax.rem(z, 2) * 4 + lax.rem(lax.div(z, 2), 2) * 2 + lax.div(z, 4)

    def xdev(d):
        return {"sp": z * NX + lax.rem(x + d, NX), "dp": dp}

    def zat(p):
        return {"sp": p * NX + x, "dp": dp}

    def ydev(d):
        return {"sp": sp, "dp": lax.rem(y + d + NY, NY) * 2 + c}

    mate = {"sp": sp, "dp": y * 2 + (1 - c)}

    def remote(src, dst, ssem, rsem, dev):
        return pltpu.make_async_remote_copy(
            src_ref=src, dst_ref=dst, send_sem=ssem, recv_sem=rsem,
            device_id=dev, device_id_type=MESH,
        )

    barrier = pltpu.get_barrier_semaphore()
    peers = [xdev(d) for d in range(1, NX)] + [ydev(1), ydev(-1), mate]
    for dev in peers:
        pl.semaphore_signal(barrier, inc=1, device_id=dev, device_id_type=MESH)
    for d in range(1, NZ):

        @pl.when(z + d < NZ)
        def _():
            dev = zat(lax.rem(z + d, NZ))
            pl.semaphore_signal(barrier, inc=1, device_id=dev, device_id_type=MESH)

    loads = [
        (i_hbm, iv, 0), (f_hbm, fv, 1), (k_hbm, kv, 2), (v_hbm, vv, 2), (w_hbm, wall.at[c, 0], 2), (q_hbm, qv, 2),
        (c_hbm, cv, 3), (n_hbm, nv, 4), (level_hbm, level, 5), (gain_hbm, gain, 6),
    ]
    for src, dst, k in loads:
        pltpu.make_async_copy(src, dst, lsem.at[k]).start()

    rows64 = lax.broadcasted_iota(jnp.int32, (T, T), 0)
    cols64 = lax.broadcasted_iota(jnp.int32, (T, T), 1)
    upper = jnp.where(rows64 <= cols64, 1.0, 0.0).astype(F32)
    causal = rows64 >= cols64

    def gates(li, f):
        li, f = li.astype(F32), f.astype(F32)
        lf = jnp.minimum(f, 0.0) - jnp.log1p(jnp.exp(-jnp.abs(f)))
        b = jnp.dot(lf, upper, precision=lax.Precision.HIGHEST, preferred_element_type=F32)
        return li - b, b[:, T - 1 : T]

    def arrived(ref, sem):
        pltpu.make_async_copy(ref, ref, sem).wait()

    with jax.named_scope("loads"):
        arrived(iv, lsem.at[0])
        arrived(fv, lsem.at[1])
    for j in range(S):
        a, _ = gates(iv[j], fv[j])
        a_loc[8 * j : 8 * j + 8, :] = a

    def block_gates(p, li, f):
        a, e = gates(li, f)
        am = jnp.max(a, axis=1, keepdims=True)
        esum[p] = jnp.broadcast_to(e, (H, D))
        amax[p] = jnp.broadcast_to(am, (H, D))
        wrow[p] = jnp.exp(a - am)

    block_gates(x, iv[x], fv[x])
    arrived(wall.at[c, 0:4], lsem.at[2])
    for k, ref in ((3, cv), (4, nv), (5, level), (6, gain)):
        arrived(ref, lsem.at[k])
    cx[x] = cv[x]
    nx[x] = nv[x]

    with jax.named_scope("barrier"):
        pl.semaphore_wait(barrier, len(peers) + z)
    for d in range(1, NZ):

        @pl.when(z >= d)
        def _():
            dev = zat(lax.rem(z - d + NZ, NZ))
            pl.semaphore_signal(hello, inc=1, device_id=dev, device_id_type=MESH)

    def rows_of(side, kind):
        if kind == "b":
            return pl.ds(pl.multiple_of(RA + RB * x, RB), RB)
        if kind == "half":
            return pl.ds(pl.multiple_of(RA + RB * x + side * (RB // 2), RB // 2), RB // 2)
        if kind == "cut":
            return pl.ds(256 + 128 * side, 128)
        return pl.ds(256 * (2 - kind if side else kind), 256)

    ring = [(0, "b"), (0, 0), (1, "b"), (0, 1), (2, "b"), (0, 2), (3, "half")]
    ring += [(1, 0), (1, 1), (1, 2), (2, 0), (2, 1), (2, 2), (3, 0), (3, "cut")]
    onward = {(0, "b"): (1, "b"), (1, "b"): (2, "b"), (2, "b"): (3, "half"), (2, 1): (3, "cut")}
    for k in range(3):
        onward[0, k], onward[1, k] = (1, k), (2, k)
    onward[2, 0] = (3, 0)

    def wsend(side, item):
        level, kind = item
        k = ring.index(item)
        rows = rows_of(side, kind)
        src, dst = (level, level + 1) if side else ((NY - level) % NY, NY - 1 - level)
        return remote(
            wall.at[c, src, rows], wall.at[c, dst, rows],
            sent.at[12], wy_r.at[k], ydev(-1 if side else 1),
        )

    def wmate(side, item):
        level, kind = item
        ref = wall.at[c, level + 1 if side else NY - 1 - level, rows_of(side, kind)]
        return remote(ref, ref, sent.at[13], wd_r.at[max(0, level - 1)], mate)

    def serve(level, kind):
        item = (level, kind)
        count = {"b": RB, "half": RB // 2, "cut": 128}.get(kind, 256)
        with jax.named_scope(f"serve{level}{kind}"):
            arrived(wall.at[c, 0:2, 0:count], wy_r.at[ring.index(item)])
        for side in (0, 1):
            if item in onward:
                wsend(side, onward[item]).start()
            if kind not in ("b", "half"):
                wmate(side, item).start()

    def begin(level, kind):
        for side in (0, 1):
            wsend(side, (level, kind)).start()

    def wspread(k):
        side, far = k % 2, k // 2
        to = xdev(NX - 1 if side else 1)
        if far:
            own = lax.rem(x + (1 if side else NX - 1), NX)
            rows = pl.ds(pl.multiple_of(RA + RB * own + side * (RB // 2), RB // 2), RB // 2)
        else:
            rows = pl.ds(pl.multiple_of(RA + RB * x, RB), RB)
        ref = wall.at[c, 1:NY, rows]
        return remote(ref, ref, sent.at[14], ws_r.at[far], to)

    def wrest():
        ref = wall.at[c, 1:NY, RA:1024]
        return remote(ref, ref, sent.at[15], ws_r.at[2], mate)

    small = [(iv, ix), (fv, fx), (cv, cx), (nv, nx)]

    def xsmall(d):
        p = lax.rem(x + d, NX)
        return [
            remote(src.at[p], dst.at[x], sent.at[k], xs_r.at[k], xdev(d)) for k, (src, dst) in enumerate(small)
        ]

    def xkeys(d, g):
        p = lax.rem(x + d, NX)
        heads = pl.ds(g * HG, HG)
        return [
            remote(src.at[p, heads], dst.at[x, heads], sent.at[4], xk_r.at[k, g], xdev(d))
            for k, (src, dst) in enumerate([(kv, kx), (vv, vx)])
        ]

    begin(0, "b")
    begin(0, 0)
    for d in (2, 1, 3):
        for copy in xsmall(d):
            copy.start()
    for g in range(G):
        for d in (2, 1, 3):
            for copy in xkeys(d, g):
                copy.start()
    remote(wall.at[c, 0], wall.at[c, 0], sent.at[15], wo_r.at[0], mate).start()

    def intra(i):
        j, h = lax.div(i, H), lax.rem(i, H)
        arow = a_loc[pl.ds(i, 1), :]
        masked = jnp.where(causal, jnp.broadcast_to(arow, (T, T)), NEG)
        top = jnp.max(masked, axis=1, keepdims=True)
        weight = jnp.exp(masked - top)
        scores = nt(qv[j, h], kv[j, h]) * FACTOR * weight
        den_s[i] = jnp.broadcast_to(jnp.sum(scores, axis=1, keepdims=True), (T, D))
        amx_s[i] = jnp.broadcast_to(top, (T, D))
        num_s[i] = jnp.dot(scores.astype(BF16), vv[j, h], preferred_element_type=F32)

    def inner(part):
        def body(i, _):
            for u in range(4):
                intra(part * 8 + i * 4 + u)
            return 0

        with jax.named_scope("intra"):
            lax.fori_loop(0, 2, body, 0)

    def state(p, h, keys, values):
        w = wrow[p, pl.ds(h, 1), :]
        vt = values[p, h].astype(F32).T
        hi = w.astype(BF16)
        lo = (w - hi.astype(F32)).astype(BF16)
        rid = lax.broadcasted_iota(jnp.int32, (16, T), 0)
        extra = jnp.where(
            rid == 0,
            jnp.broadcast_to(hi.astype(F32), (16, T)),
            jnp.where(rid == 1, jnp.broadcast_to(lo.astype(F32), (16, T)), 0.0),
        )
        lhs = jnp.concatenate([(vt * w).astype(BF16), extra.astype(BF16)], axis=0)
        st = jnp.dot(lhs, keys[p, h], preferred_element_type=F32)
        kvs[p, h] = st[0:D]
        nkv[p, pl.ds(h, 1), :] = st[D : D + 1] + st[D + 1 : D + 2]

    def states(p, g):
        with jax.named_scope("states"):
            for u in range(HG):
                state(p, g * HG + u, kx, vx)

    inner(0)

    def own(i, _):
        for u in range(4):
            state(x, i * 4 + u, kv, vv)
        return 0

    lax.fori_loop(0, 2, own, 0)
    serve(0, "b")
    begin(0, 1)
    with jax.named_scope("xgates"):
        for k, (src, dst) in enumerate(small):
            arrived(dst.at[0:3], xs_r.at[k])
        for d in (1, 3, 2):
            p = lax.rem(x - d + NX, NX)
            block_gates(p, ix[p], fx[p])

    shift = []
    before = jnp.zeros((H, D), F32)
    top = None
    for i in range(NX):
        a = amax[i] - before
        shift.append(a)
        top = a if top is None else jnp.maximum(top, a)
        before = before + esum[i]
    scale = [jnp.exp(a - top) for a in shift]

    def tz(h):
        p = rev(h)
        d = lax.rem(p - z + NZ, NZ)
        return d, [
            remote(tm_send.at[h], tm_recv.at[z], sent.at[5], tz_r.at[0], zat(p)),
            remote(t_send.at[h], t_recv.at[z], sent.at[6], tz_r.at[1], zat(p)),
        ]

    def total(g):
        with jax.named_scope(f"xin{g}"):
            for k, ref in enumerate((kx, vx)):
                arrived(ref.at[0:3, 0:HG], xk_r.at[k, g])
        for d in (1, 3, 2):
            states(lax.rem(x - d + NX, NX), g)
        for h in range(g * HG, g * HG + HG):
            ntot = sum(scale[i][h : h + 1] * nkv[i, h : h + 1, :] for i in range(NX))
            t_send[h] = sum(scale[i][h : h + 1] * kvs[i, h] for i in range(NX)).astype(BF16)
            tm_send[h, 0:1, :] = ntot
            tm_send[h, 1:2, :] = before[h : h + 1]
            tm_send[h, 2:3, :] = top[h : h + 1]
            tm_send[h, 3:4, :] = nfirst[h : h + 1]

    def total_send(g):
        for h in range(g * HG, g * HG + HG):
            d, copies = tz(h)

            @pl.when(d != 0)
            def _():
                for copy in copies:
                    copy.start()

    def cz(d):
        p = lax.rem(z + d, NZ)
        h = lax.rem(p, 2) * 4 + lax.rem(lax.div(p, 2), 2) * 2 + lax.div(p, 4)
        return remote(cz_send.at[h], cz_recv.at[z], sent.at[7], tz_r.at[2], zat(p))

    for i in range(NX):
        turn[4 * i : 4 * i + 4, 0:H] = nx[i]
        for h in range(H):
            cz_send[h, 4 * i : 4 * i + 4, :] = cx[i, 4 * h : 4 * h + 4, :]
    first_lanes = lax.broadcasted_iota(jnp.int32, (H, D), 1) < 4 * NX
    nfirst = jnp.where(first_lanes, turn[...].T[0:H], 0.0)

    group = lax.div(mine, HG)

    def pz(d):
        p = lax.rem(z + d, NZ)
        return [
            remote(pm_send.at[p], pm_recv.at[mine], sent.at[8], pz_r.at[0, group], zat(p)),
            remote(p_send.at[p], p_recv.at[mine], sent.at[9], pz_r.at[1, group], zat(p)),
        ]

    def scan(g):
        @pl.when(group == g)
        def _():
            with jax.named_scope(f"zin{g}"):
                for k, ref in enumerate((tm_recv, t_recv, cz_recv)):
                    arrived(ref.at[0 : NZ - 1], tz_r.at[k])
            with jax.named_scope("scan"):
                t_recv[z] = t_send[mine]
                tm_recv[z] = tm_send[mine]
                cz_recv[z] = cz_send[mine]
                lanes = lax.broadcasted_iota(jnp.int32, (1, H), 1)
                m = jnp.sum(jnp.where(lanes == mine, level[pl.ds(x, 1), :], 0.0), axis=1, keepdims=True)
                m = jnp.broadcast_to(m, (1, D))
                nrow = tm_recv[0, 3:4, :]
                for i in range(1, NZ):
                    nrow = nrow + pltpu.roll(tm_recv[i, 3:4, :], 4 * NX * i, 1)
                cur = jnp.concatenate([cz_recv[i] for i in range(NZ)], axis=0).T
                for i in range(NZ):
                    p_send[i] = cur.astype(BF16)
                    pm_send[i, 0:1, :] = nrow
                    pm_send[i, 1:2, :] = m
                    am = tm_recv[i, 2:3, :]
                    hi = jnp.maximum(m, am)
                    keep, add = jnp.exp(m - hi), jnp.exp(am - hi)
                    cur = keep * cur + add * t_recv[i].astype(F32)
                    nrow = keep * nrow + add * tm_recv[i, 0:1, :]
                    m = tm_recv[i, 1:2, :] + hi
                for d in (4, 3, 5, 2, 6, 1, 7):
                    for copy in pz(d):
                        copy.start()
                p_recv[mine] = p_send[z]
                pm_recv[mine] = pm_send[z]

    def xo(d, g):
        p = lax.rem(x + d, NX)
        heads = pl.ds(g * HG, HG)
        return [
            remote(bm_send.at[p, g], bm_recv.at[x, g], sent.at[10], xo_r.at[0, g], xdev(d)),
            remote(b_send.at[p, heads], b_recv.at[x, heads], sent.at[11], xo_r.at[1, g], xdev(d)),
        ]

    def spread(g):
        with jax.named_scope(f"zout{g}"):

            @pl.when(group == g)
            def _():
                for k, ref in enumerate((pm_recv, p_recv)):
                    arrived(ref.at[0 : HG - 1], pz_r.at[k, g])

            @pl.when(group != g)
            def _():
                for k, ref in enumerate((pm_recv, p_recv)):
                    arrived(ref.at[0:HG], pz_r.at[k, g])

        for u in range(HG):
            h = g * HG + u
            cur = p_recv[h].astype(F32)
            nrow = pm_recv[h, 0:1, :]
            m = pm_recv[h, 1:2, :]
            for i in range(NX):
                b_send[i, h] = cur.astype(BF16)
                bm_send[i, g, 2 * u : 2 * u + 1, :] = nrow
                bm_send[i, g, 2 * u + 1 : 2 * u + 2, :] = m
                if i < NX - 1:
                    am = amax[i, h : h + 1, :]
                    hi = jnp.maximum(m, am)
                    keep, add = jnp.exp(m - hi), jnp.exp(am - hi)
                    cur = keep * cur + add * kvs[i, h]
                    nrow = keep * nrow + add * nkv[i, h : h + 1, :]
                    m = esum[i, h : h + 1, :] + hi
        for d in (2, 1, 3):
            for copy in xo(d, g):
                copy.start()
        heads = pl.ds(g * HG, HG)
        b_recv[x, heads] = b_send[x, heads]
        bm_recv[x, g] = bm_send[x, g]

    def finish_one(j, g):
        for u in range(HG):
            h = g * HG + u
            i = j * H + h
            q = qv[j, h]
            nrow = bm_recv[j, g, 2 * u : 2 * u + 1, :]
            m = bm_recv[j, g, 2 * u + 1 : 2 * u + 2, :]
            qc = nt(q, b_recv[j, h])
            qn = jnp.sum(q.astype(F32) * nrow, axis=1, keepdims=True)
            a = amx_s[i]
            hi = jnp.maximum(a, m)
            keep, add = jnp.exp(m - hi) * FACTOR, jnp.exp(a - hi)
            den = add * den_s[i] + keep * qn
            num = add * num_s[i] + keep * qc
            o = (num / jnp.maximum(jnp.abs(den), 1.0)).astype(BF16)
            normed = (o.astype(F32) * gain[h : h + 1, :]).astype(BF16)
            hid[pl.ds(pl.multiple_of(j * T, T), T), h * D : h * D + D] = normed

    def finish(g):
        with jax.named_scope("finish"):
            finish_one(x, g)
        with jax.named_scope(f"xout{g}"):
            arrived(bm_recv.at[0:3, 0], xo_r.at[0, g])
            arrived(b_recv.at[0:3, 0:HG], xo_r.at[1, g])
        with jax.named_scope("finish"):
            for d in (1, 3, 2):
                finish_one(lax.rem(x - d + NX, NX), g)

    def columns(core, r):
        block = lax.rem(y + r, NY) * 2 + core
        return pl.ds(pl.multiple_of(block * 256, 256), 256)

    def early_one(r):
        for core in (0, 1):
            acc[core, r] = jnp.dot(hid[:, 0:RA], wall[core, r, 0:RA], preferred_element_type=F32)

    def late_one(r):
        for core in (0, 1):
            part = jnp.dot(hid[:, RA:1024], wall[core, r, RA:1024], preferred_element_type=F32)
            out[:, columns(core, r)] = (acc[core, r] + part).astype(BF16)

    def twos(name, fn, low, high):
        def body(i, _):
            fn(lax.rem(NY - 2 + 2 * i, NY))
            fn(lax.rem(NY - 1 + 2 * i, NY))
            return 0

        with jax.named_scope(name):
            lax.fori_loop(low, high, body, 0)

    def last():
        with jax.named_scope("last"):
            for core in (0, 1):
                whole = jnp.dot(hid[...], wall[core, NY // 2], preferred_element_type=F32)
                out[:, columns(core, NY // 2)] = whole.astype(BF16)

    def mates(level):
        with jax.named_scope("mate"):
            count = (4, 2, 1)[level]
            arrived(wall.at[c, 0:count, 0:RA], wd_r.at[level])

    def zgate():
        with jax.named_scope("zgate"):

            @pl.when(z < NZ - 1)
            def _():
                pl.semaphore_wait(hello, NZ - 1 - z)

    def cz_all():
        for d in (4, 3, 5, 2, 6, 1, 7):
            cz(d).start()

    def wspread_near():
        with jax.named_scope("wspread"):
            arrived(wall.at[c, 1:NY, 0 : 2 * RB], ws_r.at[0])
        wspread(2).start()
        wspread(3).start()

    def wspread_far():
        with jax.named_scope("wspread"):
            arrived(wall.at[c, 1:NY, 0:RB], ws_r.at[1])
        wrest().start()

    def sent_cell():
        for k, ref in enumerate((iv, fv, cv, nv)):
            arrived(ref.at[0:3], sent.at[k])
        arrived(b_send.at[0:3], sent.at[4])
        for k, ref in ((5, tm_send), (6, t_send), (7, cz_send), (8, pm_send), (9, p_send)):
            arrived(ref.at[0 : NZ - 1], sent.at[k])
        arrived(wall.at[c, 1:NY, 0 : 3 * RB], sent.at[14])

    def sent_rest():
        arrived(bm_send.at[0:3], sent.at[10])
        arrived(b_send.at[0:3], sent.at[11])
        arrived(wall.at[c, :, 0:352], sent.at[15])

    def sent_ring():
        arrived(wall.at[c, 1:NY, 0:832], sent.at[12])
        arrived(wall.at[c, 1:NY, 0:768], sent.at[13])

    inner(1)
    total(0)
    serve(1, "b")
    begin(0, 2)

    @pl.when(z < NZ // 2)
    def _():
        inner(2)
        total(1)
        zgate()
        total_send(0)
        cz_all()
        total_send(1)
        serve(2, "b")
        serve(0, 0)
        serve(0, 1)
        inner(3)
        total(2)
        total_send(2)
        serve(3, "half")
        wspread(0).start()
        wspread(1).start()
        serve(0, 2)
        total(3)
        total_send(3)
        serve(1, 0)
        serve(1, 1)
        wspread_near()
        scan(0)
        serve(1, 2)
        scan(1)
        wspread_far()
        serve(2, 0)
        scan(2)
        spread(0)
        serve(2, 1)
        scan(3)
        spread(1)
        serve(2, 2)
        finish(0)
        spread(2)
        finish(1)
        serve(3, 0)
        serve(3, "cut")
        spread(3)
        arrived(wall.at[c, 0], wo_r.at[0])
        mates(0)
        mates(1)
        mates(2)
        finish(2)
        twos("early", early_one, 0, 4)
        sent_cell()
        finish(3)
        arrived(wall.at[c, 1:NY, RA:1024], ws_r.at[2])
        twos("late", late_one, 0, 4)
        sent_rest()
        sent_ring()

    @pl.when(z >= NZ // 2)
    def _():
        zgate()
        total_send(0)
        cz_all()
        inner(2)
        total(1)
        total_send(1)
        serve(2, "b")
        serve(0, 0)
        serve(0, 1)
        inner(3)
        total(2)
        total_send(2)
        serve(3, "half")
        wspread(0).start()
        wspread(1).start()
        scan(0)
        serve(0, 2)
        total(3)
        total_send(3)
        scan(1)
        serve(1, 0)
        spread(0)
        serve(1, 1)
        wspread_near()
        scan(2)
        spread(1)
        serve(1, 2)
        scan(3)
        finish(0)
        serve(2, 0)
        spread(2)
        finish(1)
        serve(2, 1)
        spread(3)
        wspread_far()
        arrived(wall.at[c, 0], wo_r.at[0])
        mates(0)
        finish(2)
        twos("early", early_one, 0, 2)
        serve(2, 2)
        sent_cell()
        finish(3)
        mates(1)
        with jax.named_scope("early"):
            early_one(2)
            early_one(3)
            early_one(5)
        serve(3, 0)
        arrived(wall.at[c, 1:NY, RA:1024], ws_r.at[2])
        twos("late", late_one, 0, 3)
        with jax.named_scope("late"):
            late_one(5)
        serve(3, "cut")
        sent_rest()
        mates(2)
        last()
        sent_ring()

def on_device(queries, keys, values, input_gate, forget_gate, start_memory, start_norm, start_level, head_gain, out_weight):
    arrays = (
        input_gate, forget_gate, queries, keys, values, start_memory.reshape(S, 32, D),
        jnp.transpose(start_norm, (0, 2, 1)), out_weight, start_level, head_gain,
    )
    dma, vmem = pltpu.SemaphoreType.DMA, pltpu.VMEM
    out = pl.pallas_call(
        kernel,
        out_shape=pltpu.VMEM((S * T, 4096), BF16),
        in_specs=[pl.BlockSpec(memory_space=pltpu.HBM)] * len(arrays),
        out_specs=pl.BlockSpec(memory_space=pltpu.VMEM),
        scratch_shapes=[
            vmem((S, H, T, D), BF16), vmem((S, H, T, D), BF16), vmem((S, H, T, D), BF16),
            vmem((S, H, T), BF16), vmem((S, H, T), BF16), vmem((S, 32, D), F32), vmem((S, 4, H), F32),
            vmem((NX, H, T, D), BF16), vmem((NX, H, T, D), BF16),
            vmem((NX, H, T), BF16), vmem((NX, H, T), BF16), vmem((NX, 32, D), F32), vmem((NX, 4, H), F32),
            vmem((S, H), F32), vmem((H, D), F32),
            vmem((2, NY, 1024, 256), BF16),
            vmem((S * H, T), F32),
            vmem((S * H, T, D), F32), vmem((S * H, T, D), F32), vmem((S * H, T, D), F32),
            vmem((NX, H, T), F32), vmem((NX, H, D), F32), vmem((NX, H, D), F32),
            vmem((NX, H, D, D), F32), vmem((NX, H, D), F32), vmem((D, D), F32),
            vmem((H, 16, D), F32), vmem((NZ, 16, D), F32),
            vmem((H, D, D), BF16), vmem((NZ, D, D), BF16),
            vmem((H, 8, D), F32), vmem((NZ, 8, D), F32),
            vmem((NZ, D, D), BF16), vmem((H, D, D), BF16),
            vmem((NZ, 8, D), F32), vmem((H, 8, D), F32),
            vmem((NX, H, D, D), BF16), vmem((S, H, D, D), BF16),
            vmem((NX, G, 8, D), F32), vmem((S, G, 8, D), F32),
            vmem((S * T, H * D), BF16), vmem((2, NY, S * T, 256), F32),
            dma((7,)), dma((16,)), dma((4,)), dma((2, G)), dma((3,)), dma((2, G)), dma((2, G)),
            dma((15,)), dma((3,)), dma((3,)), dma((1,)), pltpu.SemaphoreType.REGULAR,
        ],
        compiler_params=pltpu.CompilerParams(
            collective_id=0, has_side_effects=True, vmem_limit_bytes=50_000_000
        ),
        name="cell_layer",
    )(*(pltpu.with_memory_space_constraint(array, pltpu.HBM) for array in arrays))
    return out.reshape(S, T, 4096)


def solution(mesh):
    return jax.shard_map(
        on_device,
        mesh=mesh,
        in_specs=(
            P("dp", None, "sp", None),
            P("dp", None, "sp", None),
            P("dp", None, "sp", None),
            P("dp", None, "sp"),
            P("dp", None, "sp"),
            P("dp", None, "sp", None),
            P("dp", None, "sp"),
            P("dp", None),
            P(),
            P(None, "dp"),
        ),
        out_specs=P("dp", "sp", None),
        check_vma=False,
    )
```

time: 62.3 us -> 53.4 us (0.86)
  Pallas kernels: 60.8 us -> 52 us
    pallas_call x1, Pallas kernels: 60.8 us -> 52 us  [on_device(): pl.pallas_call(kernel, out_shape=pltpu.VMEM((S * T, 4096), BF16), in_spec...]
where the time goes in v4:
time: 53.4 us; the launch traced here: 53.3 us
  Pallas kernels  52 us (97%)
  local copies, waits for them, and re-layouts  1.32 us (2%)
    pallas_call x1, Pallas kernels, on_device(): pl.pallas_call(kernel, out_shape=pltpu.VMEM((S * T, 4096), BF16), in_spec...  52 us
    unnamed x1, local copies, waits for them, and re-layouts  1.32 us

profile of v4, /device:TPU:1, one launch (start us, length us, event | category | flops | bytes accessed | tf_op | source)
XLA Modules:
  0.0 53.3 jit_solution(9374672475052591845)
XLA Ops:
  0.0 52.0 %cell_layer.1 = bf16[256,4096]{1,0:T(8,128)(2,1)S(1)} custom-call(bf16[4,8,64]{2,1,0:T(8,128)(2,1)} %i_hbm.1, bf16[4,8,64]{2,1,0:T(8,128)(2,1)} %f_hbm.1, bf16[4,8,64,128]{3,2,1,0:T(8,128)(2,1)} %q_hbm.1, bf16[4,8,64,128]{3,2,1,0:T(8,128)(2,1)} %k_hbm.1, bf16[4,8,64,128]{3,2,1,0:T(8,128)(2,1)} %v_hbm.1, f32[4,32,128]{2,1,0:T(8,128)} %bitcast.4, ...), custom_call_target="tpu_custom_call" | custom-call | tf_op jit(solution)/shard_map/cell_layer/pallas_call | solution.py:630
  52.0 1.3 %copy.12 = bf16[4,64,4096]{2,1,0:T(8,128)(2,1)} copy(bf16[4,64,4096]{2,1,0:T(8,128)(2,1)S(1)} %bitcast.3) | data formatting | bytes 4194304

commit v5 on v4

--- a/solution.py
+++ b/solution.py
@@ -12,6 +12,7 @@
 NX, NZ, NY = 4, 8, 8
 FACTOR = D**-0.5
 NEG = -1e30
+FEW = 3
 G = 4
 HG = H // G
 RA = 768
@@ -29,7 +30,7 @@
 def kernel(
     i_hbm, f_hbm, q_hbm, k_hbm, v_hbm, c_hbm, n_hbm, w_hbm, level_hbm, gain_hbm, out,
     qv, kv, vv, iv, fv, cv, nv, kx, vx, ix, fx, cx, nx, level, gain, wall, a_loc, num_s, den_s, amx_s,
-    wrow, esum, amax, kvs, nkv, turn, cz_send, cz_recv, t_send, t_recv, tm_send, tm_recv,
+    wrow, esum, amax, kvs, nkv, turn, cz_send, cz_recv, held, held_n, t_send, t_recv, tm_send, tm_recv,
     p_send, p_recv, pm_send, pm_recv, b_send, b_recv, bm_send, bm_recv, hid, acc,
     lsem, sent, xs_r, xk_r, tz_r, pz_r, xo_r, wy_r, wd_r, ws_r, wo_r, hello,
 ):
@@ -164,16 +165,10 @@
         for side in (0, 1):
             wsend(side, (level, kind)).start()
 
-    def wspread(k):
-        side, far = k % 2, k // 2
-        to = xdev(NX - 1 if side else 1)
-        if far:
-            own = lax.rem(x + (1 if side else NX - 1), NX)
-            rows = pl.ds(pl.multiple_of(RA + RB * own + side * (RB // 2), RB // 2), RB // 2)
-        else:
-            rows = pl.ds(pl.multiple_of(RA + RB * x, RB), RB)
+    def wspread(d):
+        rows = pl.ds(pl.multiple_of(RA + RB * x, RB), RB)
         ref = wall.at[c, 1:NY, rows]
-        return remote(ref, ref, sent.at[14], ws_r.at[far], to)
+        return remote(ref, ref, sent.at[14], ws_r.at[0], xdev(d))
 
     def wrest():
         ref = wall.at[c, 1:NY, RA:1024]
@@ -274,12 +269,14 @@
         before = before + esum[i]
     scale = [jnp.exp(a - top) for a in shift]
 
+    half = jnp.minimum(lax.div(z, FEW), 1)
+
     def tz(h):
         p = rev(h)
         d = lax.rem(p - z + NZ, NZ)
         return d, [
-            remote(tm_send.at[h], tm_recv.at[z], sent.at[5], tz_r.at[0], zat(p)),
-            remote(t_send.at[h], t_recv.at[z], sent.at[6], tz_r.at[1], zat(p)),
+            remote(tm_send.at[h], tm_recv.at[z], sent.at[5], tz_r.at[0, half], zat(p)),
+            remote(t_send.at[h], t_recv.at[z], sent.at[6], tz_r.at[1, half], zat(p)),
         ]
 
     def total(g):
@@ -294,7 +291,6 @@
             tm_send[h, 0:1, :] = ntot
             tm_send[h, 1:2, :] = before[h : h + 1]
             tm_send[h, 2:3, :] = top[h : h + 1]
-            tm_send[h, 3:4, :] = nfirst[h : h + 1]
 
     def total_send(g):
         for h in range(g * HG, g * HG + HG):
@@ -308,7 +304,7 @@
     def cz(d):
         p = lax.rem(z + d, NZ)
         h = lax.rem(p, 2) * 4 + lax.rem(lax.div(p, 2), 2) * 2 + lax.div(p, 4)
-        return remote(cz_send.at[h], cz_recv.at[z], sent.at[7], tz_r.at[2], zat(p))
+        return remote(cz_send.at[h], cz_recv.at[z], sent.at[7], tz_r.at[2, 0], zat(p))
 
     for i in range(NX):
         turn[4 * i : 4 * i + 4, 0:H] = nx[i]
@@ -316,22 +312,59 @@
             cz_send[h, 4 * i : 4 * i + 4, :] = cx[i, 4 * h : 4 * h + 4, :]
     first_lanes = lax.broadcasted_iota(jnp.int32, (H, D), 1) < 4 * NX
     nfirst = jnp.where(first_lanes, turn[...].T[0:H], 0.0)
+    for h in range(H):
+        cz_send[h, 16:17, :] = nfirst[h : h + 1]
 
     group = lax.div(mine, HG)
 
-    def pz(d):
-        p = lax.rem(z + d, NZ)
-        return [
-            remote(pm_send.at[p], pm_recv.at[mine], sent.at[8], pz_r.at[0, group], zat(p)),
-            remote(p_send.at[p], p_recv.at[mine], sent.at[9], pz_r.at[1, group], zat(p)),
-        ]
-
-    def scan(g):
+    def scan_states(low, high, cur, nrow, m):
+        for i in range(low, high):
+            p_send[i] = cur.astype(BF16)
+            pm_send[i, 0:1, :] = nrow
+            pm_send[i, 1:2, :] = m
+            if i == FEW:
+                held[...] = cur
+                held_n[0:1, :] = nrow
+                held_n[1:2, :] = m
+            if i < high - 1:
+                cur, nrow, m = scan_step(i, cur, nrow, m)
+        for p in range(low, high):
+
+            @pl.when(z != p)
+            def _():
+                remote(pm_send.at[p], pm_recv.at[mine], sent.at[8], pz_r.at[0, group], zat(p)).start()
+                remote(p_send.at[p], p_recv.at[mine], sent.at[9], pz_r.at[1, group], zat(p)).start()
+
+            @pl.when(z == p)
+            def _():
+                p_recv[mine] = p_send[p]
+                pm_recv[mine] = pm_send[p]
+
+    def scan_step(i, cur, nrow, m):
+        am = tm_recv[i, 2:3, :]
+        hi = jnp.maximum(m, am)
+        keep, add = jnp.exp(m - hi), jnp.exp(am - hi)
+        cur = keep * cur + add * t_recv[i].astype(F32)
+        nrow = keep * nrow + add * tm_recv[i, 0:1, :]
+        return cur, nrow, tm_recv[i, 1:2, :] + hi
+
+    def totals_wait(k, count):
+        @pl.when(half == k)
+        def _():
+            arrived(tm_recv.at[0 : count - 1], tz_r.at[0, k])
+            arrived(t_recv.at[0 : count - 1], tz_r.at[1, k])
+
+        @pl.when(half != k)
+        def _():
+            arrived(tm_recv.at[0:count], tz_r.at[0, k])
+            arrived(t_recv.at[0:count], tz_r.at[1, k])
+
+    def scan_low(g):
         @pl.when(group == g)
         def _():
-            with jax.named_scope(f"zin{g}"):
-                for k, ref in enumerate((tm_recv, t_recv, cz_recv)):
-                    arrived(ref.at[0 : NZ - 1], tz_r.at[k])
+            with jax.named_scope(f"zlow{g}"):
+                arrived(cz_recv.at[0 : NZ - 1], tz_r.at[2, 0])
+                totals_wait(0, FEW)
             with jax.named_scope("scan"):
                 t_recv[z] = t_send[mine]
                 tm_recv[z] = tm_send[mine]
@@ -339,25 +372,20 @@
                 lanes = lax.broadcasted_iota(jnp.int32, (1, H), 1)
                 m = jnp.sum(jnp.where(lanes == mine, level[pl.ds(x, 1), :], 0.0), axis=1, keepdims=True)
                 m = jnp.broadcast_to(m, (1, D))
-                nrow = tm_recv[0, 3:4, :]
+                nrow = cz_recv[0, 16:17, :]
                 for i in range(1, NZ):
-                    nrow = nrow + pltpu.roll(tm_recv[i, 3:4, :], 4 * NX * i, 1)
-                cur = jnp.concatenate([cz_recv[i] for i in range(NZ)], axis=0).T
-                for i in range(NZ):
-                    p_send[i] = cur.astype(BF16)
-                    pm_send[i, 0:1, :] = nrow
-                    pm_send[i, 1:2, :] = m
-                    am = tm_recv[i, 2:3, :]
-                    hi = jnp.maximum(m, am)
-                    keep, add = jnp.exp(m - hi), jnp.exp(am - hi)
-                    cur = keep * cur + add * t_recv[i].astype(F32)
-                    nrow = keep * nrow + add * tm_recv[i, 0:1, :]
-                    m = tm_recv[i, 1:2, :] + hi
-                for d in (4, 3, 5, 2, 6, 1, 7):
-                    for copy in pz(d):
-                        copy.start()
-                p_recv[mine] = p_send[z]
-                pm_recv[mine] = pm_send[z]
+                    nrow = nrow + pltpu.roll(cz_recv[i, 16:17, :], 4 * NX * i, 1)
+                cur = jnp.concatenate([cz_recv[i, 0:16, :] for i in range(NZ)], axis=0).T
+                scan_states(0, FEW + 1, cur, nrow, m)
+
+    def scan_high(g):
+        @pl.when(group == g)
+        def _():
+            with jax.named_scope(f"zhigh{g}"):
+                totals_wait(1, NZ - FEW)
+            with jax.named_scope("scan"):
+                state = scan_step(FEW, held[...], held_n[0:1, :], held_n[1:2, :])
+                scan_states(FEW + 1, NZ, *state)
 
     def xo(d, g):
         p = lax.rem(x + d, NX)
@@ -475,15 +503,13 @@
         for d in (4, 3, 5, 2, 6, 1, 7):
             cz(d).start()
 
-    def wspread_near():
+    def wspread_start():
+        for d in (2, 1, 3):
+            wspread(d).start()
+
+    def wspread_done():
         with jax.named_scope("wspread"):
-            arrived(wall.at[c, 1:NY, 0 : 2 * RB], ws_r.at[0])
-        wspread(2).start()
-        wspread(3).start()
-
-    def wspread_far():
-        with jax.named_scope("wspread"):
-            arrived(wall.at[c, 1:NY, 0:RB], ws_r.at[1])
+            arrived(wall.at[c, 1:NY, 0 : 3 * RB], ws_r.at[0])
         wrest().start()
 
     def sent_cell():
@@ -503,18 +529,23 @@
         arrived(wall.at[c, 1:NY, 0:832], sent.at[12])
         arrived(wall.at[c, 1:NY, 0:768], sent.at[13])
 
+    @pl.when(z >= NZ // 2)
+    def _():
+        zgate()
+        cz_all()
+
     inner(1)
-    total(0)
     serve(1, "b")
     begin(0, 2)
+    total(0)
 
     @pl.when(z < NZ // 2)
     def _():
         inner(2)
         total(1)
         zgate()
+        cz_all()
         total_send(0)
-        cz_all()
         total_send(1)
         serve(2, "b")
         serve(0, 0)
@@ -523,49 +554,48 @@
         total(2)
         total_send(2)
         serve(3, "half")
-        wspread(0).start()
-        wspread(1).start()
+        wspread_start()
         serve(0, 2)
         total(3)
         total_send(3)
+        scan_low(0)
+        scan_low(1)
         serve(1, 0)
+        scan_low(2)
+        scan_low(3)
+        scan_high(0)
         serve(1, 1)
-        wspread_near()
-        scan(0)
+        scan_high(1)
+        spread(0)
         serve(1, 2)
-        scan(1)
-        wspread_far()
+        scan_high(2)
+        scan_high(3)
+        spread(1)
         serve(2, 0)
-        scan(2)
-        spread(0)
+        spread(2)
+        wspread_done()
+        finish(0)
         serve(2, 1)
-        scan(3)
-        spread(1)
-        serve(2, 2)
-        finish(0)
-        spread(2)
-        finish(1)
-        serve(3, 0)
-        serve(3, "cut")
         spread(3)
         arrived(wall.at[c, 0], wo_r.at[0])
+        sent_cell()
+        finish(1)
         mates(0)
+        serve(2, 2)
+        finish(2)
+        twos("early", early_one, 0, 2)
+        serve(3, 0)
         mates(1)
-        mates(2)
-        finish(2)
-        twos("early", early_one, 0, 4)
-        sent_cell()
+        with jax.named_scope("early"):
+            early_one(2)
+            early_one(3)
+            early_one(5)
+        serve(3, "cut")
         finish(3)
-        arrived(wall.at[c, 1:NY, RA:1024], ws_r.at[2])
-        twos("late", late_one, 0, 4)
-        sent_rest()
-        sent_ring()
 
     @pl.when(z >= NZ // 2)
     def _():
-        zgate()
         total_send(0)
-        cz_all()
         inner(2)
         total(1)
         total_send(1)
@@ -573,53 +603,57 @@
         serve(0, 0)
         serve(0, 1)
         inner(3)
+        scan_low(0)
         total(2)
         total_send(2)
         serve(3, "half")
-        wspread(0).start()
-        wspread(1).start()
-        scan(0)
+        wspread_start()
+        scan_low(1)
+        scan_high(0)
         serve(0, 2)
         total(3)
         total_send(3)
-        scan(1)
+        scan_low(2)
+        scan_high(1)
         serve(1, 0)
+        scan_low(3)
         spread(0)
+        scan_high(2)
         serve(1, 1)
-        wspread_near()
-        scan(2)
+        scan_high(3)
         spread(1)
         serve(1, 2)
-        scan(3)
+        spread(2)
+        serve(2, 0)
         finish(0)
-        serve(2, 0)
-        spread(2)
+        spread(3)
+        wspread_done()
+        serve(2, 1)
         finish(1)
-        serve(2, 1)
-        spread(3)
-        wspread_far()
         arrived(wall.at[c, 0], wo_r.at[0])
         mates(0)
+        serve(2, 2)
         finish(2)
         twos("early", early_one, 0, 2)
-        serve(2, 2)
         sent_cell()
-        finish(3)
+        serve(3, 0)
         mates(1)
         with jax.named_scope("early"):
             early_one(2)
             early_one(3)
             early_one(5)
-        serve(3, 0)
-        arrived(wall.at[c, 1:NY, RA:1024], ws_r.at[2])
-        twos("late", late_one, 0, 3)
-        with jax.named_scope("late"):
-            late_one(5)
+        finish(3)
         serve(3, "cut")
-        sent_rest()
-        mates(2)
-        last()
-        sent_ring()
+
+    arrived(wall.at[c, 1:NY, RA:1024], ws_r.at[2])
+    twos("late", late_one, 0, 3)
+    with jax.named_scope("late"):
+        late_one(5)
+    sent_rest()
+    mates(2)
+    last()
+    sent_ring()
+
 
 def on_device(queries, keys, values, input_gate, forget_gate, start_memory, start_norm, start_level, head_gain, out_weight):
     arrays = (
@@ -643,7 +677,7 @@
             vmem((S * H, T, D), F32), vmem((S * H, T, D), F32), vmem((S * H, T, D), F32),
             vmem((NX, H, T), F32), vmem((NX, H, D), F32), vmem((NX, H, D), F32),
             vmem((NX, H, D, D), F32), vmem((NX, H, D), F32), vmem((D, D), F32),
-            vmem((H, 16, D), F32), vmem((NZ, 16, D), F32),
+            vmem((H, 24, D), F32), vmem((NZ, 24, D), F32), vmem((D, D), F32), vmem((8, D), F32),
             vmem((H, D, D), BF16), vmem((NZ, D, D), BF16),
             vmem((H, 8, D), F32), vmem((NZ, 8, D), F32),
             vmem((NZ, D, D), BF16), vmem((H, D, D), BF16),
@@ -651,7 +685,7 @@
             vmem((NX, H, D, D), BF16), vmem((S, H, D, D), BF16),
             vmem((NX, G, 8, D), F32), vmem((S, G, 8, D), F32),
             vmem((S * T, H * D), BF16), vmem((2, NY, S * T, 256), F32),
-            dma((7,)), dma((16,)), dma((4,)), dma((2, G)), dma((3,)), dma((2, G)), dma((2, G)),
+            dma((7,)), dma((16,)), dma((4,)), dma((2, G)), dma((3, 2)), dma((2, G)), dma((2, G)),
             dma((15,)), dma((3,)), dma((3,)), dma((1,)), pltpu.SemaphoreType.REGULAR,
         ],
         compiler_params=pltpu.CompilerParams(

time: 53.4 us -> 49.2 us (0.921); the launches traced: 53.3 us -> 48.4 us
  Pallas kernels: 52 us -> 47 us
    pallas_call x1, Pallas kernels: 52 us -> 47 us  [on_device(): pl.pallas_call(kernel, out_shape=pltpu.VMEM((S * T, 4096), BF16), in_spec...]
where the time goes in v5:
time: 49.2 us; the launch traced here: 48.4 us
  Pallas kernels  47 us (96%)
  local copies, waits for them, and re-layouts  1.32 us (3%)
    pallas_call x1, Pallas kernels, on_device(): pl.pallas_call(kernel, out_shape=pltpu.VMEM((S * T, 4096), BF16), in_spec...  47 us
    unnamed x1, local copies, waits for them, and re-layouts  1.32 us

profile of v5, /device:TPU:1, one launch (start us, length us, event | category | flops | bytes accessed | tf_op | source)
XLA Modules:
  0.0 48.4 jit_solution(3648312970390966207)
XLA Ops:
  0.0 47.0 %cell_layer.1 = bf16[256,4096]{1,0:T(8,128)(2,1)S(1)} custom-call(bf16[4,8,64]{2,1,0:T(8,128)(2,1)} %i_hbm.1, bf16[4,8,64]{2,1,0:T(8,128)(2,1)} %f_hbm.1, bf16[4,8,64,128]{3,2,1,0:T(8,128)(2,1)} %q_hbm.1, bf16[4,8,64,128]{3,2,1,0:T(8,128)(2,1)} %k_hbm.1, bf16[4,8,64,128]{3,2,1,0:T(8,128)(2,1)} %v_hbm.1, f32[4,32,128]{2,1,0:T(8,128)} %bitcast.4, ...), custom_call_target="tpu_custom_call" | custom-call | tf_op jit(solution)/shard_map/cell_layer/pallas_call | solution.py:664
  47.0 1.3 %copy.12 = bf16[4,64,4096]{2,1,0:T(8,128)(2,1)} copy(bf16[4,64,4096]{2,1,0:T(8,128)(2,1)S(1)} %bitcast.3) | data formatting | bytes 4194304

commit v6 on v5

--- a/solution.py
+++ b/solution.py
@@ -12,7 +12,6 @@
 NX, NZ, NY = 4, 8, 8
 FACTOR = D**-0.5
 NEG = -1e30
-FEW = 3
 G = 4
 HG = H // G
 RA = 768
@@ -23,23 +22,17 @@
     return lax.dot_general(a, b, (((1,), (1,)), ((), ())), preferred_element_type=F32)
 
 
-def rev(i):
-    return i % 2 * 4 + i // 2 % 2 * 2 + i // 4
-
-
 def kernel(
     i_hbm, f_hbm, q_hbm, k_hbm, v_hbm, c_hbm, n_hbm, w_hbm, level_hbm, gain_hbm, out,
     qv, kv, vv, iv, fv, cv, nv, kx, vx, ix, fx, cx, nx, level, gain, wall, a_loc, num_s, den_s, amx_s,
-    wrow, esum, amax, kvs, nkv, turn, cz_send, cz_recv, held, held_n, t_send, t_recv, tm_send, tm_recv,
+    wrow, esum, amax, kvs, nkv, turn, cz_send, cz_recv, nz_send, nz_recv, first_c, first_n, tot, ntot,
     p_send, p_recv, pm_send, pm_recv, b_send, b_recv, bm_send, bm_recv, hid, acc,
-    lsem, sent, xs_r, xk_r, tz_r, pz_r, xo_r, wy_r, wd_r, ws_r, wo_r, hello,
+    lsem, sent, xs_r, xk_r, tz_r, pz_r, xo_r, wy_r, wd_r, ws_r, wo_r, hello, hello_next,
 ):
     sp = lax.axis_index("sp")
     dp = lax.axis_index("dp")
     x, z = lax.rem(sp, NX), lax.div(sp, NX)
     y, c = lax.div(dp, 2), lax.rem(dp, 2)
-    mine = lax.rem(z, 2) * 4 + lax.rem(lax.div(z, 2), 2) * 2 + lax.div(z, 4)
-
     def xdev(d):
         return {"sp": z * NX + lax.rem(x + d, NX), "dp": dp}
 
@@ -118,6 +111,8 @@
         def _():
             dev = zat(lax.rem(z - d + NZ, NZ))
             pl.semaphore_signal(hello, inc=1, device_id=dev, device_id_type=MESH)
+            if d == 1:
+                pl.semaphore_signal(hello_next, inc=1, device_id=dev, device_id_type=MESH)
 
     def rows_of(side, kind):
         if kind == "b":
@@ -269,15 +264,7 @@
         before = before + esum[i]
     scale = [jnp.exp(a - top) for a in shift]
 
-    half = jnp.minimum(lax.div(z, FEW), 1)
-
-    def tz(h):
-        p = rev(h)
-        d = lax.rem(p - z + NZ, NZ)
-        return d, [
-            remote(tm_send.at[h], tm_recv.at[z], sent.at[5], tz_r.at[0, half], zat(p)),
-            remote(t_send.at[h], t_recv.at[z], sent.at[6], tz_r.at[1, half], zat(p)),
-        ]
+    lanes = lax.broadcasted_iota(jnp.int32, (1, H), 1)
 
     def total(g):
         with jax.named_scope(f"xin{g}"):
@@ -286,106 +273,88 @@
         for d in (1, 3, 2):
             states(lax.rem(x - d + NX, NX), g)
         for h in range(g * HG, g * HG + HG):
-            ntot = sum(scale[i][h : h + 1] * nkv[i, h : h + 1, :] for i in range(NX))
-            t_send[h] = sum(scale[i][h : h + 1] * kvs[i, h] for i in range(NX)).astype(BF16)
-            tm_send[h, 0:1, :] = ntot
-            tm_send[h, 1:2, :] = before[h : h + 1]
-            tm_send[h, 2:3, :] = top[h : h + 1]
-
-    def total_send(g):
-        for h in range(g * HG, g * HG + HG):
-            d, copies = tz(h)
-
-            @pl.when(d != 0)
-            def _():
-                for copy in copies:
-                    copy.start()
+            ntot[h : h + 1, :] = sum(scale[i][h : h + 1] * nkv[i, h : h + 1, :] for i in range(NX))
+            tot[h] = sum(scale[i][h : h + 1] * kvs[i, h] for i in range(NX))
 
     def cz(d):
         p = lax.rem(z + d, NZ)
-        h = lax.rem(p, 2) * 4 + lax.rem(lax.div(p, 2), 2) * 2 + lax.div(p, 4)
-        return remote(cz_send.at[h], cz_recv.at[z], sent.at[7], tz_r.at[2, 0], zat(p))
+        return [
+            remote(cz_send, cz_recv.at[z], sent.at[5], tz_r.at[0], zat(p)),
+            remote(nz_send, nz_recv.at[z], sent.at[6], tz_r.at[1], zat(p)),
+        ]
 
     for i in range(NX):
         turn[4 * i : 4 * i + 4, 0:H] = nx[i]
         for h in range(H):
-            cz_send[h, 4 * i : 4 * i + 4, :] = cx[i, 4 * h : 4 * h + 4, :]
+            turn[16 + 16 * h + 4 * i : 20 + 16 * h + 4 * i, :] = cx[i, 4 * h : 4 * h + 4, :]
     first_lanes = lax.broadcasted_iota(jnp.int32, (H, D), 1) < 4 * NX
-    nfirst = jnp.where(first_lanes, turn[...].T[0:H], 0.0)
+    nz_send[...] = jnp.where(first_lanes, turn[0:D, :].T[0:H], 0.0)
     for h in range(H):
-        cz_send[h, 16:17, :] = nfirst[h : h + 1]
-
-    group = lax.div(mine, HG)
-
-    def scan_states(low, high, cur, nrow, m):
-        for i in range(low, high):
-            p_send[i] = cur.astype(BF16)
-            pm_send[i, 0:1, :] = nrow
-            pm_send[i, 1:2, :] = m
-            if i == FEW:
-                held[...] = cur
-                held_n[0:1, :] = nrow
-                held_n[1:2, :] = m
-            if i < high - 1:
-                cur, nrow, m = scan_step(i, cur, nrow, m)
-        for p in range(low, high):
-
-            @pl.when(z != p)
-            def _():
-                remote(pm_send.at[p], pm_recv.at[mine], sent.at[8], pz_r.at[0, group], zat(p)).start()
-                remote(p_send.at[p], p_recv.at[mine], sent.at[9], pz_r.at[1, group], zat(p)).start()
-
-            @pl.when(z == p)
-            def _():
-                p_recv[mine] = p_send[p]
-                pm_recv[mine] = pm_send[p]
-
-    def scan_step(i, cur, nrow, m):
-        am = tm_recv[i, 2:3, :]
-        hi = jnp.maximum(m, am)
-        keep, add = jnp.exp(m - hi), jnp.exp(am - hi)
-        cur = keep * cur + add * t_recv[i].astype(F32)
-        nrow = keep * nrow + add * tm_recv[i, 0:1, :]
-        return cur, nrow, tm_recv[i, 1:2, :] + hi
-
-    def totals_wait(k, count):
-        @pl.when(half == k)
+        cz_send[h] = turn[16 + 16 * h : 32 + 16 * h, :].astype(BF16)
+
+    def pz(h):
+        return [
+            remote(pm_send.at[h], pm_recv.at[h], sent.at[8], pz_r.at[0, h], zat(lax.rem(z + 1, NZ))),
+            remote(p_send.at[h], p_recv.at[h], sent.at[9], pz_r.at[1, h], zat(lax.rem(z + 1, NZ))),
+        ]
+
+    def first(g):
+        @pl.when(z == 0)
         def _():
-            arrived(tm_recv.at[0 : count - 1], tz_r.at[0, k])
-            arrived(t_recv.at[0 : count - 1], tz_r.at[1, k])
-
-        @pl.when(half != k)
+            if g == 0:
+                pl.semaphore_wait(hello_next, 1)
+            for h in range(g * HG, g * HG + HG):
+                p_send[h] = tot[h].astype(BF16)
+                pm_send[h, 0:1, :] = ntot[h : h + 1, :]
+                pm_send[h, 1:2, :] = before[h : h + 1] + top[h : h + 1]
+                pm_send[h, 2:3, :] = before[h : h + 1]
+                p_recv[h] = jnp.zeros((D, D), BF16)
+                pm_recv[h] = jnp.where(small_rows == 1, NEG, 0.0)
+            for h in range(g * HG, g * HG + HG):
+                for copy in pz(h):
+                    copy.start()
+
+    small_rows = lax.broadcasted_iota(jnp.int32, (8, D), 0)
+
+    def chain(g):
+        @pl.when(z > 0)
         def _():
-            arrived(tm_recv.at[0:count], tz_r.at[0, k])
-            arrived(t_recv.at[0:count], tz_r.at[1, k])
-
-    def scan_low(g):
-        @pl.when(group == g)
-        def _():
-            with jax.named_scope(f"zlow{g}"):
-                arrived(cz_recv.at[0 : NZ - 1], tz_r.at[2, 0])
-                totals_wait(0, FEW)
-            with jax.named_scope("scan"):
-                t_recv[z] = t_send[mine]
-                tm_recv[z] = tm_send[mine]
-                cz_recv[z] = cz_send[mine]
-                lanes = lax.broadcasted_iota(jnp.int32, (1, H), 1)
-                m = jnp.sum(jnp.where(lanes == mine, level[pl.ds(x, 1), :], 0.0), axis=1, keepdims=True)
-                m = jnp.broadcast_to(m, (1, D))
-                nrow = cz_recv[0, 16:17, :]
-                for i in range(1, NZ):
-                    nrow = nrow + pltpu.roll(cz_recv[i, 16:17, :], 4 * NX * i, 1)
-                cur = jnp.concatenate([cz_recv[i, 0:16, :] for i in range(NZ)], axis=0).T
-                scan_states(0, FEW + 1, cur, nrow, m)
-
-    def scan_high(g):
-        @pl.when(group == g)
-        def _():
-            with jax.named_scope(f"zhigh{g}"):
-                totals_wait(1, NZ - FEW)
-            with jax.named_scope("scan"):
-                state = scan_step(FEW, held[...], held_n[0:1, :], held_n[1:2, :])
-                scan_states(FEW + 1, NZ, *state)
+            if g == 0:
+
+                @pl.when(z < NZ - 1)
+                def _():
+                    pl.semaphore_wait(hello_next, 1)
+
+            for h in range(g * HG, g * HG + HG):
+                with jax.named_scope(f"chain{g}"):
+                    arrived(pm_recv.at[h], pz_r.at[0, h])
+                    arrived(p_recv.at[h], pz_r.at[1, h])
+
+                @pl.when(z < NZ - 1)
+                def _():
+                    m = pm_recv[h, 1:2, :]
+                    hi = jnp.maximum(m, top[h : h + 1])
+                    keep, add = jnp.exp(m - hi), jnp.exp(top[h : h + 1] - hi)
+                    p_send[h] = (keep * p_recv[h].astype(F32) + add * tot[h]).astype(BF16)
+                    pm_send[h, 0:1, :] = keep * pm_recv[h, 0:1, :] + add * ntot[h : h + 1, :]
+                    pm_send[h, 1:2, :] = before[h : h + 1] + hi
+                    pm_send[h, 2:3, :] = before[h : h + 1] + pm_recv[h, 2:3, :]
+                    for copy in pz(h):
+                        copy.start()
+
+    def starts():
+        with jax.named_scope("zstart"):
+            arrived(cz_recv.at[0 : NZ - 1], tz_r.at[0])
+            arrived(nz_recv.at[0 : NZ - 1], tz_r.at[1])
+        with jax.named_scope("starts"):
+            cz_recv[z] = cz_send[...]
+            nz_recv[z] = nz_send[...]
+            rows = nz_recv[0]
+            for i in range(1, NZ):
+                rows = rows + pltpu.roll(nz_recv[i], 4 * NX * i, 1)
+            first_n[...] = rows
+            for h in range(H):
+                first_c[h] = jnp.concatenate([cz_recv[i, h].astype(F32) for i in range(NZ)], axis=0).T
 
     def xo(d, g):
         p = lax.rem(x + d, NX)
@@ -396,23 +365,16 @@
         ]
 
     def spread(g):
-        with jax.named_scope(f"zout{g}"):
-
-            @pl.when(group == g)
-            def _():
-                for k, ref in enumerate((pm_recv, p_recv)):
-                    arrived(ref.at[0 : HG - 1], pz_r.at[k, g])
-
-            @pl.when(group != g)
-            def _():
-                for k, ref in enumerate((pm_recv, p_recv)):
-                    arrived(ref.at[0:HG], pz_r.at[k, g])
-
         for u in range(HG):
             h = g * HG + u
-            cur = p_recv[h].astype(F32)
-            nrow = pm_recv[h, 0:1, :]
-            m = pm_recv[h, 1:2, :]
+            m = jnp.sum(jnp.where(lanes == h, level[pl.ds(x, 1), :], 0.0), axis=1, keepdims=True)
+            m = m + pm_recv[h, 2:3, :]
+            come = pm_recv[h, 1:2, :]
+            hi = jnp.maximum(m, come)
+            keep, add = jnp.exp(m - hi), jnp.exp(come - hi)
+            cur = keep * first_c[h] + add * p_recv[h].astype(F32)
+            nrow = keep * first_n[h : h + 1, :] + add * pm_recv[h, 0:1, :]
+            m = hi
             for i in range(NX):
                 b_send[i, h] = cur.astype(BF16)
                 bm_send[i, g, 2 * u : 2 * u + 1, :] = nrow
@@ -501,7 +463,8 @@
 
     def cz_all():
         for d in (4, 3, 5, 2, 6, 1, 7):
-            cz(d).start()
+            for copy in cz(d):
+                copy.start()
 
     def wspread_start():
         for d in (2, 1, 3):
@@ -516,8 +479,14 @@
         for k, ref in enumerate((iv, fv, cv, nv)):
             arrived(ref.at[0:3], sent.at[k])
         arrived(b_send.at[0:3], sent.at[4])
-        for k, ref in ((5, tm_send), (6, t_send), (7, cz_send), (8, pm_send), (9, p_send)):
-            arrived(ref.at[0 : NZ - 1], sent.at[k])
+        arrived(cz_recv.at[0 : NZ - 1], sent.at[5])
+        arrived(nz_recv.at[0 : NZ - 1], sent.at[6])
+
+        @pl.when(z < NZ - 1)
+        def _():
+            arrived(pm_send, sent.at[8])
+            arrived(p_send, sent.at[9])
+
         arrived(wall.at[c, 1:NY, 0 : 3 * RB], sent.at[14])
 
     def sent_rest():
@@ -541,49 +510,47 @@
 
     @pl.when(z < NZ // 2)
     def _():
+        first(0)
         inner(2)
         total(1)
+        first(1)
         zgate()
         cz_all()
-        total_send(0)
-        total_send(1)
         serve(2, "b")
         serve(0, 0)
         serve(0, 1)
         inner(3)
+        chain(0)
         total(2)
-        total_send(2)
+        first(2)
         serve(3, "half")
         wspread_start()
+        chain(1)
         serve(0, 2)
         total(3)
-        total_send(3)
-        scan_low(0)
-        scan_low(1)
+        first(3)
+        chain(2)
         serve(1, 0)
-        scan_low(2)
-        scan_low(3)
-        scan_high(0)
+        starts()
+        spread(0)
+        chain(3)
+        spread(1)
         serve(1, 1)
-        scan_high(1)
-        spread(0)
+        spread(2)
+        spread(3)
         serve(1, 2)
-        scan_high(2)
-        scan_high(3)
-        spread(1)
+        finish(0)
+        wspread_done()
         serve(2, 0)
-        spread(2)
-        wspread_done()
-        finish(0)
+        finish(1)
+        sent_cell()
+        arrived(wall.at[c, 0], wo_r.at[0])
         serve(2, 1)
-        spread(3)
-        arrived(wall.at[c, 0], wo_r.at[0])
-        sent_cell()
-        finish(1)
         mates(0)
+        finish(2)
         serve(2, 2)
-        finish(2)
         twos("early", early_one, 0, 2)
+        finish(3)
         serve(3, 0)
         mates(1)
         with jax.named_scope("early"):
@@ -591,58 +558,95 @@
             early_one(3)
             early_one(5)
         serve(3, "cut")
-        finish(3)
-
-    @pl.when(z >= NZ // 2)
+
+    @pl.when(jnp.logical_and(z >= NZ // 2, z < NZ - 2))
     def _():
-        total_send(0)
         inner(2)
         total(1)
-        total_send(1)
         serve(2, "b")
         serve(0, 0)
         serve(0, 1)
         inner(3)
-        scan_low(0)
         total(2)
-        total_send(2)
         serve(3, "half")
         wspread_start()
-        scan_low(1)
-        scan_high(0)
         serve(0, 2)
         total(3)
-        total_send(3)
-        scan_low(2)
-        scan_high(1)
+        starts()
         serve(1, 0)
-        scan_low(3)
+        chain(0)
         spread(0)
-        scan_high(2)
+        chain(1)
         serve(1, 1)
-        scan_high(3)
         spread(1)
+        chain(2)
         serve(1, 2)
         spread(2)
+        chain(3)
+        spread(3)
+        finish(0)
         serve(2, 0)
-        finish(0)
-        spread(3)
         wspread_done()
+        finish(1)
         serve(2, 1)
-        finish(1)
+        sent_cell()
         arrived(wall.at[c, 0], wo_r.at[0])
         mates(0)
+        finish(2)
         serve(2, 2)
-        finish(2)
         twos("early", early_one, 0, 2)
-        sent_cell()
+        finish(3)
         serve(3, 0)
         mates(1)
         with jax.named_scope("early"):
             early_one(2)
             early_one(3)
             early_one(5)
+        serve(3, "cut")
+
+    @pl.when(z >= NZ - 2)
+    def _():
+        inner(2)
+        total(1)
+        serve(2, "b")
+        serve(0, 0)
+        serve(0, 1)
+        inner(3)
+        total(2)
+        serve(3, "half")
+        wspread_start()
+        serve(0, 2)
+        total(3)
+        starts()
+        serve(1, 0)
+        serve(1, 1)
+        chain(0)
+        spread(0)
+        serve(1, 2)
+        chain(1)
+        spread(1)
+        serve(2, 0)
+        chain(2)
+        spread(2)
+        serve(2, 1)
+        finish(0)
+        chain(3)
+        spread(3)
+        wspread_done()
+        serve(2, 2)
+        finish(1)
+        sent_cell()
+        arrived(wall.at[c, 0], wo_r.at[0])
+        mates(0)
+        finish(2)
+        twos("early", early_one, 0, 2)
+        serve(3, 0)
         finish(3)
+        mates(1)
+        with jax.named_scope("early"):
+            early_one(2)
+            early_one(3)
+            early_one(5)
         serve(3, "cut")
 
     arrived(wall.at[c, 1:NY, RA:1024], ws_r.at[2])
@@ -676,17 +680,16 @@
             vmem((S * H, T), F32),
             vmem((S * H, T, D), F32), vmem((S * H, T, D), F32), vmem((S * H, T, D), F32),
             vmem((NX, H, T), F32), vmem((NX, H, D), F32), vmem((NX, H, D), F32),
-            vmem((NX, H, D, D), F32), vmem((NX, H, D), F32), vmem((D, D), F32),
-            vmem((H, 24, D), F32), vmem((NZ, 24, D), F32), vmem((D, D), F32), vmem((8, D), F32),
-            vmem((H, D, D), BF16), vmem((NZ, D, D), BF16),
-            vmem((H, 8, D), F32), vmem((NZ, 8, D), F32),
-            vmem((NZ, D, D), BF16), vmem((H, D, D), BF16),
-            vmem((NZ, 8, D), F32), vmem((H, 8, D), F32),
+            vmem((NX, H, D, D), F32), vmem((NX, H, D), F32), vmem((16 + D, D), F32),
+            vmem((H, 16, D), BF16), vmem((NZ, H, 16, D), BF16), vmem((H, D), F32), vmem((NZ, H, D), F32),
+            vmem((H, D, D), F32), vmem((H, D), F32), vmem((H, D, D), F32), vmem((H, D), F32),
+            vmem((H, D, D), BF16), vmem((H, D, D), BF16),
+            vmem((H, 8, D), F32), vmem((H, 8, D), F32),
             vmem((NX, H, D, D), BF16), vmem((S, H, D, D), BF16),
             vmem((NX, G, 8, D), F32), vmem((S, G, 8, D), F32),
             vmem((S * T, H * D), BF16), vmem((2, NY, S * T, 256), F32),
-            dma((7,)), dma((16,)), dma((4,)), dma((2, G)), dma((3, 2)), dma((2, G)), dma((2, G)),
-            dma((15,)), dma((3,)), dma((3,)), dma((1,)), pltpu.SemaphoreType.REGULAR,
+            dma((7,)), dma((16,)), dma((4,)), dma((2, G)), dma((2,)), dma((2, H)), dma((2, G)),
+            dma((15,)), dma((3,)), dma((3,)), dma((1,)), pltpu.SemaphoreType.REGULAR, pltpu.SemaphoreType.REGULAR,
         ],
         compiler_params=pltpu.CompilerParams(
             collective_id=0, has_side_effects=True, vmem_limit_bytes=50_000_000

time: 49.2 us -> 52.5 us (1.067)
  the two profiles are of different devices: /device:TPU:1 before, /device:TPU:217 now
where the time goes in v6:
time: 52.5 us; the launch traced here: 52.3 us
  Pallas kernels  51 us (97%)
  local copies, waits for them, and re-layouts  1.32 us (3%)
    pallas_call x1, Pallas kernels, on_device(): pl.pallas_call(kernel, out_shape=pltpu.VMEM((S * T, 4096), BF16), in_spec...  51 us
    unnamed x1, local copies, waits for them, and re-layouts  1.32 us

profile of v6, /device:TPU:217, one launch (start us, length us, event | category | flops | bytes accessed | tf_op | source)
XLA Modules:
  0.0 52.3 jit_solution(17827308838570968376)
XLA Ops:
  0.0 51.0 %cell_layer.1 = bf16[256,4096]{1,0:T(8,128)(2,1)S(1)} custom-call(bf16[4,8,64]{2,1,0:T(8,128)(2,1)} %i_hbm.1, bf16[4,8,64]{2,1,0:T(8,128)(2,1)} %f_hbm.1, bf16[4,8,64,128]{3,2,1,0:T(8,128)(2,1)} %q_hbm.1, bf16[4,8,64,128]{3,2,1,0:T(8,128)(2,1)} %k_hbm.1, bf16[4,8,64,128]{3,2,1,0:T(8,128)(2,1)} %v_hbm.1, f32[4,32,128]{2,1,0:T(8,128)} %bitcast.4, ...), custom_call_target="tpu_custom_call" | custom-call | tf_op jit(solution)/shard_map/cell_layer/pallas_call | solution.py:668
  51.0 1.3 %copy.12 = bf16[4,64,4096]{2,1,0:T(8,128)(2,1)} copy(bf16[4,64,4096]{2,1,0:T(8,128)(2,1)S(1)} %bitcast.3) | data formatting | bytes 4194304

commit v7 on v5

--- a/solution.py
+++ b/solution.py
@@ -12,7 +12,7 @@
 NX, NZ, NY = 4, 8, 8
 FACTOR = D**-0.5
 NEG = -1e30
-FEW = 3
+NQ = NZ // 2
 G = 4
 HG = H // G
 RA = 768
@@ -23,23 +23,19 @@
     return lax.dot_general(a, b, (((1,), (1,)), ((), ())), preferred_element_type=F32)
 
 
-def rev(i):
-    return i % 2 * 4 + i // 2 % 2 * 2 + i // 4
-
-
 def kernel(
     i_hbm, f_hbm, q_hbm, k_hbm, v_hbm, c_hbm, n_hbm, w_hbm, level_hbm, gain_hbm, out,
     qv, kv, vv, iv, fv, cv, nv, kx, vx, ix, fx, cx, nx, level, gain, wall, a_loc, num_s, den_s, amx_s,
-    wrow, esum, amax, kvs, nkv, turn, cz_send, cz_recv, held, held_n, t_send, t_recv, tm_send, tm_recv,
+    wrow, esum, amax, kvs, nkv, turn, cz_send, cz_recv, h_send, h_recv, hm_send, hm_recv, t_send, t_recv, tm_send, tm_recv,
     p_send, p_recv, pm_send, pm_recv, b_send, b_recv, bm_send, bm_recv, hid, acc,
-    lsem, sent, xs_r, xk_r, tz_r, pz_r, xo_r, wy_r, wd_r, ws_r, wo_r, hello,
+    lsem, sent, xs_r, xk_r, tz_r, pz_r, xo_r, wy_r, wd_r, ws_r, wo_r, hr_r, hello, hello_far,
 ):
     sp = lax.axis_index("sp")
     dp = lax.axis_index("dp")
     x, z = lax.rem(sp, NX), lax.div(sp, NX)
     y, c = lax.div(dp, 2), lax.rem(dp, 2)
-    mine = lax.rem(z, 2) * 4 + lax.rem(lax.div(z, 2), 2) * 2 + lax.div(z, 4)
-
+    zq = lax.rem(z, NQ)
+    below = z - zq
     def xdev(d):
         return {"sp": z * NX + lax.rem(x + d, NX), "dp": dp}
 
@@ -112,12 +108,16 @@
 
     with jax.named_scope("barrier"):
         pl.semaphore_wait(barrier, len(peers) + z)
-    for d in range(1, NZ):
-
-        @pl.when(z >= d)
+    for d in range(1, NQ):
+
+        @pl.when(zq >= d)
         def _():
             dev = zat(lax.rem(z - d + NZ, NZ))
             pl.semaphore_signal(hello, inc=1, device_id=dev, device_id_type=MESH)
+
+    @pl.when(z >= NQ)
+    def _():
+        pl.semaphore_signal(hello_far, inc=1, device_id=zat(lax.rem(z + NQ, NZ)), device_id_type=MESH)
 
     def rows_of(side, kind):
         if kind == "b":
@@ -269,14 +269,12 @@
         before = before + esum[i]
     scale = [jnp.exp(a - top) for a in shift]
 
-    half = jnp.minimum(lax.div(z, FEW), 1)
-
     def tz(h):
-        p = rev(h)
-        d = lax.rem(p - z + NZ, NZ)
-        return d, [
-            remote(tm_send.at[h], tm_recv.at[z], sent.at[5], tz_r.at[0, half], zat(p)),
-            remote(t_send.at[h], t_recv.at[z], sent.at[6], tz_r.at[1, half], zat(p)),
+        w = h // NQ
+        to = zat(below + h % NQ)
+        return [
+            remote(tm_send.at[h], tm_recv.at[w, zq], sent.at[5], tz_r.at[0, w], to),
+            remote(t_send.at[h], t_recv.at[w, zq], sent.at[6], tz_r.at[1, w], to),
         ]
 
     def total(g):
@@ -294,98 +292,111 @@
 
     def total_send(g):
         for h in range(g * HG, g * HG + HG):
-            d, copies = tz(h)
-
-            @pl.when(d != 0)
+            copies = tz(h)
+
+            @pl.when(jnp.logical_and(zq != h % NQ, z < NZ - 1))
             def _():
                 for copy in copies:
                     copy.start()
 
-    def cz(d):
-        p = lax.rem(z + d, NZ)
-        h = lax.rem(p, 2) * 4 + lax.rem(lax.div(p, 2), 2) * 2 + lax.div(p, 4)
-        return remote(cz_send.at[h], cz_recv.at[z], sent.at[7], tz_r.at[2, 0], zat(p))
+    def cz(o):
+        return remote(cz_send.at[o], cz_recv.at[z], sent.at[7], tz_r.at[2, 0], zat(o))
 
     for i in range(NX):
         turn[4 * i : 4 * i + 4, 0:H] = nx[i]
         for h in range(H):
-            cz_send[h, 4 * i : 4 * i + 4, :] = cx[i, 4 * h : 4 * h + 4, :]
+            at = 16 * (h // NQ) + 4 * i
+            cz_send[h % NQ, at : at + 4, :] = cx[i, 4 * h : 4 * h + 4, :]
     first_lanes = lax.broadcasted_iota(jnp.int32, (H, D), 1) < 4 * NX
     nfirst = jnp.where(first_lanes, turn[...].T[0:H], 0.0)
     for h in range(H):
-        cz_send[h, 16:17, :] = nfirst[h : h + 1]
-
-    group = lax.div(mine, HG)
-
-    def scan_states(low, high, cur, nrow, m):
-        for i in range(low, high):
-            p_send[i] = cur.astype(BF16)
-            pm_send[i, 0:1, :] = nrow
-            pm_send[i, 1:2, :] = m
-            if i == FEW:
-                held[...] = cur
-                held_n[0:1, :] = nrow
-                held_n[1:2, :] = m
-            if i < high - 1:
-                cur, nrow, m = scan_step(i, cur, nrow, m)
-        for p in range(low, high):
-
-            @pl.when(z != p)
-            def _():
-                remote(pm_send.at[p], pm_recv.at[mine], sent.at[8], pz_r.at[0, group], zat(p)).start()
-                remote(p_send.at[p], p_recv.at[mine], sent.at[9], pz_r.at[1, group], zat(p)).start()
-
-            @pl.when(z == p)
-            def _():
-                p_recv[mine] = p_send[p]
-                pm_recv[mine] = pm_send[p]
-
-    def scan_step(i, cur, nrow, m):
-        am = tm_recv[i, 2:3, :]
+        cz_send[h % NQ, 32 + h // NQ : 33 + h // NQ, :] = nfirst[h : h + 1]
+
+    def scan_step(w, i, cur, nrow, m):
+        am = tm_recv[w, i, 2:3, :]
         hi = jnp.maximum(m, am)
         keep, add = jnp.exp(m - hi), jnp.exp(am - hi)
-        cur = keep * cur + add * t_recv[i].astype(F32)
-        nrow = keep * nrow + add * tm_recv[i, 0:1, :]
-        return cur, nrow, tm_recv[i, 1:2, :] + hi
-
-    def totals_wait(k, count):
-        @pl.when(half == k)
+        cur = keep * cur + add * t_recv[w, i].astype(F32)
+        nrow = keep * nrow + add * tm_recv[w, i, 0:1, :]
+        return cur, nrow, tm_recv[w, i, 1:2, :] + hi
+
+    def scan_states(g, head, cur, nrow, m):
+        w = g // 2
+        for i in range(NQ):
+            p_send[w, i] = cur.astype(BF16)
+            pm_send[w, i, 0:1, :] = nrow
+            pm_send[w, i, 1:2, :] = m
+            if i < NQ - 1:
+                cur, nrow, m = scan_step(w, i, cur, nrow, m)
+        for i in range(NQ):
+
+            @pl.when(zq != i)
+            def _():
+                to = zat(below + i)
+                remote(pm_send.at[w, i], pm_recv.at[head], sent.at[8], pz_r.at[0, g], to).start()
+                remote(p_send.at[w, i], p_recv.at[head], sent.at[9], pz_r.at[1, g], to).start()
+
+            @pl.when(zq == i)
+            def _():
+                p_recv[head] = p_send[w, i]
+                pm_recv[head] = pm_send[w, i]
+
+        return cur, nrow, m
+
+    def totals_wait(w, count):
+        arrived(tm_recv.at[w, 0:count], tz_r.at[0, w])
+        arrived(t_recv.at[w, 0:count], tz_r.at[1, w])
+
+    runs = lax.div(zq, 2)
+
+    def scan(g):
+        w = g // 2
+        head = zq + NQ * w
+
+        @pl.when(jnp.logical_and(runs == g % 2, z < NQ))
         def _():
-            arrived(tm_recv.at[0 : count - 1], tz_r.at[0, k])
-            arrived(t_recv.at[0 : count - 1], tz_r.at[1, k])
-
-        @pl.when(half != k)
+            with jax.named_scope(f"zin{g}"):
+                if w == 0:
+                    arrived(cz_recv.at[0 : NZ - 1], tz_r.at[2, 0])
+                    cz_recv[z] = cz_send[zq]
+                    pl.semaphore_wait(hello_far, 1)
+                totals_wait(w, NQ - 1)
+            with jax.named_scope("scan"):
+                t_recv[w, zq] = t_send[head]
+                tm_recv[w, zq] = tm_send[head]
+                lanes = lax.broadcasted_iota(jnp.int32, (1, H), 1)
+                m = jnp.sum(jnp.where(lanes == head, level[pl.ds(x, 1), :], 0.0), axis=1, keepdims=True)
+                m = jnp.broadcast_to(m, (1, D))
+                nrow = cz_recv[0, 32 + w : 33 + w, :]
+                for i in range(1, NZ):
+                    nrow = nrow + pltpu.roll(cz_recv[i, 32 + w : 33 + w, :], 4 * NX * i, 1)
+                cur = jnp.concatenate([cz_recv[i, 16 * w : 16 * w + 16, :] for i in range(NZ)], axis=0).T
+                cur, nrow, m = scan_step(w, NQ - 1, *scan_states(g, head, cur, nrow, m))
+                h_send[w] = cur.astype(BF16)
+                hm_send[w, 0:1, :] = nrow
+                hm_send[w, 1:2, :] = m
+                to = zat(lax.rem(z + NQ, NZ))
+                remote(hm_send.at[w], hm_recv.at[w], sent.at[16], hr_r.at[0, w], to).start()
+                remote(h_send.at[w], h_recv.at[w], sent.at[17], hr_r.at[1, w], to).start()
+
+        @pl.when(jnp.logical_and(runs == g % 2, z >= NQ))
         def _():
-            arrived(tm_recv.at[0:count], tz_r.at[0, k])
-            arrived(t_recv.at[0:count], tz_r.at[1, k])
-
-    def scan_low(g):
-        @pl.when(group == g)
-        def _():
-            with jax.named_scope(f"zlow{g}"):
-                arrived(cz_recv.at[0 : NZ - 1], tz_r.at[2, 0])
-                totals_wait(0, FEW)
+            with jax.named_scope(f"zin{g}"):
+
+                @pl.when(z < NZ - 1)
+                def _():
+                    totals_wait(w, NQ - 2)
+
+                @pl.when(z == NZ - 1)
+                def _():
+                    totals_wait(w, NQ - 1)
+
+                arrived(hm_recv.at[w], hr_r.at[0, w])
+                arrived(h_recv.at[w], hr_r.at[1, w])
             with jax.named_scope("scan"):
-                t_recv[z] = t_send[mine]
-                tm_recv[z] = tm_send[mine]
-                cz_recv[z] = cz_send[mine]
-                lanes = lax.broadcasted_iota(jnp.int32, (1, H), 1)
-                m = jnp.sum(jnp.where(lanes == mine, level[pl.ds(x, 1), :], 0.0), axis=1, keepdims=True)
-                m = jnp.broadcast_to(m, (1, D))
-                nrow = cz_recv[0, 16:17, :]
-                for i in range(1, NZ):
-                    nrow = nrow + pltpu.roll(cz_recv[i, 16:17, :], 4 * NX * i, 1)
-                cur = jnp.concatenate([cz_recv[i, 0:16, :] for i in range(NZ)], axis=0).T
-                scan_states(0, FEW + 1, cur, nrow, m)
-
-    def scan_high(g):
-        @pl.when(group == g)
-        def _():
-            with jax.named_scope(f"zhigh{g}"):
-                totals_wait(1, NZ - FEW)
-            with jax.named_scope("scan"):
-                state = scan_step(FEW, held[...], held_n[0:1, :], held_n[1:2, :])
-                scan_states(FEW + 1, NZ, *state)
+                t_recv[w, zq] = t_send[head]
+                tm_recv[w, zq] = tm_send[head]
+                scan_states(g, head, h_recv[w].astype(F32), hm_recv[w, 0:1, :], hm_recv[w, 1:2, :])
 
     def xo(d, g):
         p = lax.rem(x + d, NX)
@@ -398,12 +409,12 @@
     def spread(g):
         with jax.named_scope(f"zout{g}"):
 
-            @pl.when(group == g)
+            @pl.when(runs == g % 2)
             def _():
                 for k, ref in enumerate((pm_recv, p_recv)):
                     arrived(ref.at[0 : HG - 1], pz_r.at[k, g])
 
-            @pl.when(group != g)
+            @pl.when(runs != g % 2)
             def _():
                 for k, ref in enumerate((pm_recv, p_recv)):
                     arrived(ref.at[0:HG], pz_r.at[k, g])
@@ -495,13 +506,17 @@
     def zgate():
         with jax.named_scope("zgate"):
 
-            @pl.when(z < NZ - 1)
+            @pl.when(zq < NQ - 1)
             def _():
-                pl.semaphore_wait(hello, NZ - 1 - z)
+                pl.semaphore_wait(hello, NQ - 1 - zq)
 
     def cz_all():
-        for d in (4, 3, 5, 2, 6, 1, 7):
-            cz(d).start()
+        for o in range(NQ):
+
+            @pl.when(z != o)
+            def _():
+                cz(o).start()
+
 
     def wspread_start():
         for d in (2, 1, 3):
@@ -516,8 +531,24 @@
         for k, ref in enumerate((iv, fv, cv, nv)):
             arrived(ref.at[0:3], sent.at[k])
         arrived(b_send.at[0:3], sent.at[4])
-        for k, ref in ((5, tm_send), (6, t_send), (7, cz_send), (8, pm_send), (9, p_send)):
-            arrived(ref.at[0 : NZ - 1], sent.at[k])
+        arrived(pm_send.at[:, 0 : NQ - 1], sent.at[8])
+        arrived(p_send.at[:, 0 : NQ - 1], sent.at[9])
+
+        @pl.when(z < NZ - 1)
+        def _():
+            arrived(tm_send.at[0 : H - 2], sent.at[5])
+            arrived(t_send.at[0 : H - 2], sent.at[6])
+
+        @pl.when(z < NQ)
+        def _():
+            arrived(cz_send.at[0 : NQ - 1], sent.at[7])
+            arrived(hm_send, sent.at[16])
+            arrived(h_send, sent.at[17])
+
+        @pl.when(z >= NQ)
+        def _():
+            arrived(cz_send, sent.at[7])
+
         arrived(wall.at[c, 1:NY, 0 : 3 * RB], sent.at[14])
 
     def sent_rest():
@@ -541,11 +572,11 @@
 
     @pl.when(z < NZ // 2)
     def _():
+        zgate()
+        total_send(0)
+        cz_all()
         inner(2)
         total(1)
-        zgate()
-        cz_all()
-        total_send(0)
         total_send(1)
         serve(2, "b")
         serve(0, 0)
@@ -558,28 +589,24 @@
         serve(0, 2)
         total(3)
         total_send(3)
-        scan_low(0)
-        scan_low(1)
+        scan(1)
+        scan(0)
         serve(1, 0)
-        scan_low(2)
-        scan_low(3)
-        scan_high(0)
+        scan(2)
         serve(1, 1)
-        scan_high(1)
+        scan(3)
         spread(0)
+        spread(1)
         serve(1, 2)
-        scan_high(2)
-        scan_high(3)
-        spread(1)
+        spread(2)
         serve(2, 0)
-        spread(2)
+        finish(0)
+        spread(3)
         wspread_done()
-        finish(0)
         serve(2, 1)
-        spread(3)
+        finish(1)
+        sent_cell()
         arrived(wall.at[c, 0], wo_r.at[0])
-        sent_cell()
-        finish(1)
         mates(0)
         serve(2, 2)
         finish(2)
@@ -603,37 +630,33 @@
         serve(0, 0)
         serve(0, 1)
         inner(3)
-        scan_low(0)
         total(2)
         total_send(2)
         serve(3, "half")
         wspread_start()
-        scan_low(1)
-        scan_high(0)
         serve(0, 2)
         total(3)
         total_send(3)
-        scan_low(2)
-        scan_high(1)
         serve(1, 0)
-        scan_low(3)
+        scan(0)
+        scan(1)
+        serve(1, 1)
         spread(0)
-        scan_high(2)
-        serve(1, 1)
-        scan_high(3)
+        scan(2)
+        scan(3)
         spread(1)
         serve(1, 2)
         spread(2)
+        finish(0)
         serve(2, 0)
-        finish(0)
         spread(3)
+        finish(1)
         wspread_done()
         serve(2, 1)
-        finish(1)
         arrived(wall.at[c, 0], wo_r.at[0])
         mates(0)
+        finish(2)
         serve(2, 2)
-        finish(2)
         twos("early", early_one, 0, 2)
         sent_cell()
         serve(3, 0)
@@ -677,16 +700,17 @@
             vmem((S * H, T, D), F32), vmem((S * H, T, D), F32), vmem((S * H, T, D), F32),
             vmem((NX, H, T), F32), vmem((NX, H, D), F32), vmem((NX, H, D), F32),
             vmem((NX, H, D, D), F32), vmem((NX, H, D), F32), vmem((D, D), F32),
-            vmem((H, 24, D), F32), vmem((NZ, 24, D), F32), vmem((D, D), F32), vmem((8, D), F32),
-            vmem((H, D, D), BF16), vmem((NZ, D, D), BF16),
-            vmem((H, 8, D), F32), vmem((NZ, 8, D), F32),
-            vmem((NZ, D, D), BF16), vmem((H, D, D), BF16),
-            vmem((NZ, 8, D), F32), vmem((H, 8, D), F32),
+            vmem((NQ, 40, D), F32), vmem((NZ, 40, D), F32),
+            vmem((2, D, D), BF16), vmem((2, D, D), BF16), vmem((2, 8, D), F32), vmem((2, 8, D), F32),
+            vmem((H, D, D), BF16), vmem((2, NQ, D, D), BF16),
+            vmem((H, 8, D), F32), vmem((2, NQ, 8, D), F32),
+            vmem((2, NQ, D, D), BF16), vmem((H, D, D), BF16),
+            vmem((2, NQ, 8, D), F32), vmem((H, 8, D), F32),
             vmem((NX, H, D, D), BF16), vmem((S, H, D, D), BF16),
             vmem((NX, G, 8, D), F32), vmem((S, G, 8, D), F32),
             vmem((S * T, H * D), BF16), vmem((2, NY, S * T, 256), F32),
-            dma((7,)), dma((16,)), dma((4,)), dma((2, G)), dma((3, 2)), dma((2, G)), dma((2, G)),
-            dma((15,)), dma((3,)), dma((3,)), dma((1,)), pltpu.SemaphoreType.REGULAR,
+            dma((7,)), dma((18,)), dma((4,)), dma((2, G)), dma((3, 2)), dma((2, G)), dma((2, G)),
+            dma((15,)), dma((3,)), dma((3,)), dma((1,)), dma((2, 2)), pltpu.SemaphoreType.REGULAR, pltpu.SemaphoreType.REGULAR,
         ],
         compiler_params=pltpu.CompilerParams(
             collective_id=0, has_side_effects=True, vmem_limit_bytes=50_000_000

time: 49.2 us -> 48.5 us (0.986); the launches traced: 48.4 us -> 48.4 us
  no operation moved by 1% of the time
where the time goes in v7:
time: 48.5 us; the launch traced here: 48.4 us
  Pallas kernels  47.1 us (97%)
  local copies, waits for them, and re-layouts  1.32 us (3%)
    pallas_call x1, Pallas kernels, on_device(): pl.pallas_call(kernel, out_shape=pltpu.VMEM((S * T, 4096), BF16), in_spec...  47.1 us
    unnamed x1, local copies, waits for them, and re-layouts  1.32 us

profile of v7, /device:TPU:1, one launch (start us, length us, event | category | flops | bytes accessed | tf_op | source)
XLA Modules:
  0.0 48.4 jit_solution(2413227891884997635)
XLA Ops:
  0.0 47.1 %cell_layer.1 = bf16[256,4096]{1,0:T(8,128)(2,1)S(1)} custom-call(bf16[4,8,64]{2,1,0:T(8,128)(2,1)} %i_hbm.1, bf16[4,8,64]{2,1,0:T(8,128)(2,1)} %f_hbm.1, bf16[4,8,64,128]{3,2,1,0:T(8,128)(2,1)} %q_hbm.1, bf16[4,8,64,128]{3,2,1,0:T(8,128)(2,1)} %k_hbm.1, bf16[4,8,64,128]{3,2,1,0:T(8,128)(2,1)} %v_hbm.1, f32[4,32,128]{2,1,0:T(8,128)} %bitcast.4, ...), custom_call_target="tpu_custom_call" | custom-call | tf_op jit(solution)/shard_map/cell_layer/pallas_call | solution.py:687
  47.1 1.3 %copy.12 = bf16[4,64,4096]{2,1,0:T(8,128)(2,1)} copy(bf16[4,64,4096]{2,1,0:T(8,128)(2,1)S(1)} %bitcast.3) | data formatting | bytes 4194304

commit v8 on v7

--- a/solution.py
+++ b/solution.py
@@ -165,10 +165,11 @@
         for side in (0, 1):
             wsend(side, (level, kind)).start()
 
-    def wspread(d):
-        rows = pl.ds(pl.multiple_of(RA + RB * x, RB), RB)
-        ref = wall.at[c, 1:NY, rows]
-        return remote(ref, ref, sent.at[14], ws_r.at[0], xdev(d))
+    def wspread(side, far):
+        own = lax.rem(x + far * (1 if side else NX - 1), NX)
+        start = pl.multiple_of(RA + RB * own + far * side * (RB // 2), RB // 2)
+        ref = wall.at[c, 1:NY, pl.ds(start, RB // 2 if far else RB)]
+        return remote(ref, ref, sent.at[14], ws_r.at[far], xdev(NX - 1 if side else 1))
 
     def wrest():
         ref = wall.at[c, 1:NY, RA:1024]
@@ -328,6 +329,10 @@
             pm_send[w, i, 1:2, :] = m
             if i < NQ - 1:
                 cur, nrow, m = scan_step(w, i, cur, nrow, m)
+        return cur, nrow, m
+
+    def scan_send(g, head):
+        w = g // 2
         for i in range(NQ):
 
             @pl.when(zq != i)
@@ -340,8 +345,6 @@
             def _():
                 p_recv[head] = p_send[w, i]
                 pm_recv[head] = pm_send[w, i]
-
-        return cur, nrow, m
 
     def totals_wait(w, count):
         arrived(tm_recv.at[w, 0:count], tz_r.at[0, w])
@@ -378,6 +381,7 @@
                 to = zat(lax.rem(z + NQ, NZ))
                 remote(hm_send.at[w], hm_recv.at[w], sent.at[16], hr_r.at[0, w], to).start()
                 remote(h_send.at[w], h_recv.at[w], sent.at[17], hr_r.at[1, w], to).start()
+                scan_send(g, head)
 
         @pl.when(jnp.logical_and(runs == g % 2, z >= NQ))
         def _():
@@ -397,6 +401,7 @@
                 t_recv[w, zq] = t_send[head]
                 tm_recv[w, zq] = tm_send[head]
                 scan_states(g, head, h_recv[w].astype(F32), hm_recv[w, 0:1, :], hm_recv[w, 1:2, :])
+                scan_send(g, head)
 
     def xo(d, g):
         p = lax.rem(x + d, NX)
@@ -519,12 +524,18 @@
 
 
     def wspread_start():
-        for d in (2, 1, 3):
-            wspread(d).start()
+        wspread(0, 0).start()
+        wspread(1, 0).start()
+
+    def wspread_near():
+        with jax.named_scope("wnear"):
+            arrived(wall.at[c, 1:NY, 0 : 2 * RB], ws_r.at[0])
+        wspread(0, 1).start()
+        wspread(1, 1).start()
 
     def wspread_done():
         with jax.named_scope("wspread"):
-            arrived(wall.at[c, 1:NY, 0 : 3 * RB], ws_r.at[0])
+            arrived(wall.at[c, 1:NY, 0:RB], ws_r.at[1])
         wrest().start()
 
     def sent_cell():
@@ -594,21 +605,22 @@
         serve(1, 0)
         scan(2)
         serve(1, 1)
+        wspread_near()
         scan(3)
         spread(0)
         spread(1)
         serve(1, 2)
         spread(2)
         serve(2, 0)
+        spread(3)
+        serve(2, 1)
         finish(0)
-        spread(3)
         wspread_done()
-        serve(2, 1)
+        sent_cell()
+        serve(2, 2)
         finish(1)
-        sent_cell()
         arrived(wall.at[c, 0], wo_r.at[0])
         mates(0)
-        serve(2, 2)
         finish(2)
         twos("early", early_one, 0, 2)
         serve(3, 0)
@@ -641,32 +653,33 @@
         scan(0)
         scan(1)
         serve(1, 1)
+        wspread_near()
         spread(0)
         scan(2)
         scan(3)
         spread(1)
         serve(1, 2)
         spread(2)
-        finish(0)
         serve(2, 0)
         spread(3)
+        serve(2, 1)
+        finish(0)
+        wspread_done()
+        sent_cell()
+        serve(2, 2)
         finish(1)
-        wspread_done()
-        serve(2, 1)
         arrived(wall.at[c, 0], wo_r.at[0])
         mates(0)
         finish(2)
-        serve(2, 2)
         twos("early", early_one, 0, 2)
-        sent_cell()
         serve(3, 0)
         mates(1)
         with jax.named_scope("early"):
             early_one(2)
             early_one(3)
             early_one(5)
+        serve(3, "cut")
         finish(3)
-        serve(3, "cut")
 
     arrived(wall.at[c, 1:NY, RA:1024], ws_r.at[2])
     twos("late", late_one, 0, 3)

time: 48.5 us -> 48.5 us (level)
  no operation moved by 1% of the time
where the time goes in v8:
time: 48.5 us; the launch traced here: 48.4 us
  Pallas kernels  47.1 us (97%)
  local copies, waits for them, and re-layouts  1.32 us (3%)
    pallas_call x1, Pallas kernels, on_device(): pl.pallas_call(kernel, out_shape=pltpu.VMEM((S * T, 4096), BF16), in_spec...  47.1 us
    unnamed x1, local copies, waits for them, and re-layouts  1.32 us

profile of v8, /device:TPU:1, one launch (start us, length us, event | category | flops | bytes accessed | tf_op | source)
XLA Modules:
  0.0 48.4 jit_solution(6021140744988440918)
XLA Ops:
  0.0 47.1 %cell_layer.1 = bf16[256,4096]{1,0:T(8,128)(2,1)S(1)} custom-call(bf16[4,8,64]{2,1,0:T(8,128)(2,1)} %i_hbm.1, bf16[4,8,64]{2,1,0:T(8,128)(2,1)} %f_hbm.1, bf16[4,8,64,128]{3,2,1,0:T(8,128)(2,1)} %q_hbm.1, bf16[4,8,64,128]{3,2,1,0:T(8,128)(2,1)} %k_hbm.1, bf16[4,8,64,128]{3,2,1,0:T(8,128)(2,1)} %v_hbm.1, f32[4,32,128]{2,1,0:T(8,128)} %bitcast.4, ...), custom_call_target="tpu_custom_call" | custom-call | tf_op jit(solution)/shard_map/cell_layer/pallas_call | solution.py:700
  47.1 1.3 %copy.12 = bf16[4,64,4096]{2,1,0:T(8,128)(2,1)} copy(bf16[4,64,4096]{2,1,0:T(8,128)(2,1)S(1)} %bitcast.3) | data formatting | bytes 4194304

commit v9 on v8

--- a/solution.py
+++ b/solution.py
@@ -333,7 +333,7 @@
 
     def scan_send(g, head):
         w = g // 2
-        for i in range(NQ):
+        for i in reversed(range(NQ)):
 
             @pl.when(zq != i)
             def _():

time: 48.5 us -> 48.6 us (level)
  no operation moved by 1% of the time
where the time goes in v9:
time: 48.6 us; the launch traced here: 48.4 us
  Pallas kernels  47.1 us (97%)
  local copies, waits for them, and re-layouts  1.32 us (3%)
    pallas_call x1, Pallas kernels, on_device(): pl.pallas_call(kernel, out_shape=pltpu.VMEM((S * T, 4096), BF16), in_spec...  47.1 us
    unnamed x1, local copies, waits for them, and re-layouts  1.32 us

profile of v9, /device:TPU:1, one launch (start us, length us, event | category | flops | bytes accessed | tf_op | source)
XLA Modules:
  0.0 48.4 jit_solution(17512600304319640325)
XLA Ops:
  0.0 47.1 %cell_layer.1 = bf16[256,4096]{1,0:T(8,128)(2,1)S(1)} custom-call(bf16[4,8,64]{2,1,0:T(8,128)(2,1)} %i_hbm.1, bf16[4,8,64]{2,1,0:T(8,128)(2,1)} %f_hbm.1, bf16[4,8,64,128]{3,2,1,0:T(8,128)(2,1)} %q_hbm.1, bf16[4,8,64,128]{3,2,1,0:T(8,128)(2,1)} %k_hbm.1, bf16[4,8,64,128]{3,2,1,0:T(8,128)(2,1)} %v_hbm.1, f32[4,32,128]{2,1,0:T(8,128)} %bitcast.4, ...), custom_call_target="tpu_custom_call" | custom-call | tf_op jit(solution)/shard_map/cell_layer/pallas_call | solution.py:700
  47.1 1.3 %copy.12 = bf16[4,64,4096]{2,1,0:T(8,128)(2,1)} copy(bf16[4,64,4096]{2,1,0:T(8,128)(2,1)S(1)} %bitcast.3) | data formatting | bytes 4194304
